TPU v7x, 32 devices: a whole 2x2x4 slice. The times are simulated.
32 devices in a mesh: sp: 8 (over z, y), tp: 4 (over x, core).
Axes of the slice: x: 2, y: 2, z: 4, core: 2. Of those that a mesh axis runs over, the one named last changes fastest.
Arguments:
- queries: bfloat16 [1024, 1280], P('sp', 'tp'), may hold values from -4000 to 4000
- latents: bfloat16 [1024, 512], P('sp'), may hold values from -6 to 6
- shared_key: bfloat16 [1024, 64], P('sp'), may hold values from -4 to 4
- expand_weight: bfloat16 [512, 1536], P(None, 'tp'), may hold values from -0.25 to 0.25
- residual: bfloat16 [1024, 2048], P('sp'), may hold values from -3 to 3
- out_weight: bfloat16 [768, 2048], replicated, may hold values from -0.21875 to 0.21875
- norm_gain: bfloat16 [2048], replicated, may hold values from 0.099609375 to 1.8984375
- gate_weight: bfloat16 [2048, 3072], P('sp', 'tp'), may hold values from -0.125 to 0.125
- value_weight: bfloat16 [2048, 3072], P('sp', 'tp'), may hold values from -0.125 to 0.125
- conv_weight: bfloat16 [3, 3072], P(None, 'tp'), may hold values from -3.5 to 3.5
- down_weight: bfloat16 [3072, 2048], P('tp', 'sp'), may hold values from -0.109375 to 0.109375
Outputs:
- output: bfloat16 [1024, 2048], P(('sp', 'tp'))
All inputs are finite; a program needn't handle non-finite values.
Results may differ from a plain program's by a relative error of at most 0.018.
Values may be sent and summed in bfloat16 or wider, within the bound.
A program may use at most 128 MiB of HBM per device.

v0:
```python
import functools

import jax
import jax.numpy as jnp
from jax import lax
from jax.experimental import pallas as pl
from jax.experimental.pallas import tpu as pltpu
from jax.sharding import PartitionSpec as P

NOPE_A = 128
VAL_A = 128
NOPE_B = 64
VAL_B = 64
ROPE = 64


def padded_2(block, sides, width):
    for axis, dim in sides:
        count = lax.axis_size(axis)
        forward = [(i, i + 1) for i in range(count - 1)]
        backward = [(target, source) for source, target in forward]
        low = lax.ppermute(
            lax.slice_in_dim(block, block.shape[dim] - width, None, axis=dim), axis, forward
        )
        high = lax.ppermute(lax.slice_in_dim(block, 0, width, axis=dim), axis, backward)
        block = jnp.concatenate([low, block, high], axis=dim)
    return block


def tables(positions, width):
    half_width = width // 2
    frequency = 10000.0 ** (-jnp.arange(half_width, dtype=jnp.float32) / half_width)
    angles = positions.astype(jnp.float32)[:, None] * frequency[None, :]
    return (jnp.cos(angles), jnp.sin(angles))


def rotate(vectors, cos_table, sine_table):
    half_width = vectors.shape[-1] // 2
    first_half = vectors[:, :half_width].astype(jnp.float32)
    second_half = vectors[:, half_width:].astype(jnp.float32)
    turned = jnp.concatenate(
        [
            first_half * cos_table - second_half * sine_table,
            second_half * cos_table + first_half * sine_table,
        ],
        axis=1,
    )
    return turned.astype(jnp.bfloat16)


def normalize(stream, norm_gain):
    stream_f = stream.astype(jnp.float32)
    scaled = stream_f * lax.rsqrt(jnp.mean(stream_f * stream_f, axis=1, keepdims=True) + 1e-06)
    return (scaled * norm_gain.astype(jnp.float32)).astype(jnp.bfloat16)


def update(running, q_content, q_turned, k_content, k_turned, values, score_scale):
    row_max, row_sum, weighted = running
    scores = (
        jnp.einsum("qd,kd->qk", q_content, k_content, preferred_element_type=jnp.float32)
        + jnp.einsum("qd,kd->qk", q_turned, k_turned, preferred_element_type=jnp.float32)
    ) * score_scale
    new_max = jnp.maximum(row_max, jnp.max(scores, axis=1))
    weights = jnp.exp(scores - new_max[:, None])
    row_sum = jnp.sum(weights, axis=1)
    weighted = jnp.dot(weights.astype(jnp.bfloat16), values, preferred_element_type=jnp.float32)
    return (new_max, row_sum, weighted)


def body(
    queries,
    latents,
    shared_key,
    expand_weight,
    residual,
    out_weight,
    norm_gain,
    gate_weight,
    value_weight,
    conv_weight,
    down_weight,
):
    tok_rows = queries.shape[0]
    q_width = NOPE_A + NOPE_B + 2 * ROPE
    kv_width = NOPE_A + VAL_A + NOPE_B + VAL_B
    positions = lax.axis_index("sp") * tok_rows + jnp.arange(tok_rows, dtype=jnp.int32)
    cos_table, sine_table = tables(positions, ROPE)
    key_turned = rotate(shared_key, cos_table, sine_table)
    scale_wide = (NOPE_A + ROPE) ** (-0.5)
    scale_narrow = (NOPE_B + ROPE) ** (-0.5)
    initial = []
    pair_index = 0
    q_base = pair_index * q_width
    rotary_base = q_base + NOPE_A + NOPE_B
    wide_content = queries[:, q_base : q_base + NOPE_A]
    narrow_content = queries[:, q_base + NOPE_A : rotary_base]
    wide_turned = rotate(queries[:, rotary_base : rotary_base + ROPE], cos_table, sine_table)
    narrow_turned = rotate(
        queries[:, rotary_base + ROPE : rotary_base + 2 * ROPE], cos_table, sine_table
    )
    query_parts = [(wide_content, wide_turned, narrow_content, narrow_turned)]
    lowest = jnp.full((tok_rows,), -1e30, jnp.float32)
    empty_sum = jnp.zeros((tok_rows,), jnp.float32)
    initial += [
        lowest,
        empty_sum,
        jnp.zeros((tok_rows, VAL_A), jnp.float32),
        lowest,
        empty_sum,
        jnp.zeros((tok_rows, VAL_B), jnp.float32),
    ]
    initial = tuple(initial)
    pieces = (
        lax.all_gather(latents, "sp", axis=0, tiled=True),
        lax.all_gather(key_turned, "sp", axis=0, tiled=True),
    )
    expanded = jnp.dot(pieces[0], expand_weight, preferred_element_type=jnp.float32).astype(
        jnp.bfloat16
    )
    turned_keys = pieces[1]
    result = []
    pair_index = 0
    wide_content, wide_turned, narrow_content, narrow_turned = query_parts[pair_index]
    kv_base = pair_index * kv_width
    narrow_base = kv_base + NOPE_A + VAL_A
    wide_keys = expanded[:, kv_base : kv_base + NOPE_A]
    wide_values = expanded[:, kv_base + NOPE_A : narrow_base]
    narrow_keys = expanded[:, narrow_base : narrow_base + NOPE_B]
    narrow_values = expanded[:, narrow_base + NOPE_B : narrow_base + NOPE_B + VAL_B]
    absorb_offset = 6 * pair_index
    result += list(
        update(
            initial[absorb_offset : absorb_offset + 3],
            wide_content,
            wide_turned,
            wide_keys,
            turned_keys,
            wide_values,
            scale_wide,
        )
    )
    result += list(
        update(
            initial[absorb_offset + 3 : absorb_offset + 6],
            narrow_content,
            narrow_turned,
            narrow_keys,
            turned_keys,
            narrow_values,
            scale_narrow,
        )
    )
    running = tuple(result)
    outputs = []
    pair_index = 0
    for group_index in range(2):
        offset = 6 * pair_index + 3 * group_index
        outputs.append((running[offset + 2] / running[offset + 1][:, None]).astype(jnp.bfloat16))
    attended = jnp.concatenate(outputs, axis=1)
    share = tok_rows // lax.axis_size("tp")
    tp_index = lax.axis_index("tp")
    all_heads = lax.all_gather(attended, "tp", axis=1, tiled=True)
    projected = jnp.dot(all_heads, out_weight, preferred_element_type=jnp.float32)
    stream = (residual.astype(jnp.float32) + projected).astype(jnp.bfloat16)
    normed = normalize(stream, norm_gain)
    stream_own = lax.dynamic_slice_in_dim(stream, tp_index * share, share, 0)
    pieces = (
        lax.all_gather(gate_weight, "sp", axis=0, tiled=True),
        lax.all_gather(value_weight, "sp", axis=0, tiled=True),
    )
    gate_sum = jnp.dot(normed, pieces[0], preferred_element_type=jnp.float32)
    value_sum = jnp.dot(normed, pieces[1], preferred_element_type=jnp.float32)
    gate_pre = gate_sum.astype(jnp.bfloat16)
    value_pre = value_sum.astype(jnp.bfloat16)
    reach = conv_weight.shape[0] // 2
    padded = padded_2(gate_pre, (("sp", 0),), reach)
    mixed_gate = jnp.zeros(gate_pre.shape, jnp.float32)
    for tap in range(conv_weight.shape[0]):
        mixed_gate = mixed_gate + padded[tap : tap + tok_rows].astype(jnp.float32) * conv_weight[
            tap
        ].astype(jnp.float32)
    active = (jax.nn.silu(mixed_gate) * value_pre.astype(jnp.float32)).astype(jnp.bfloat16)
    partial_rows = jnp.dot(
        active,
        lax.all_gather(down_weight, "sp", axis=1, tiled=True),
        preferred_element_type=jnp.float32,
    )
    summed = lax.psum_scatter(
        partial_rows.astype(jnp.bfloat16), "tp", scatter_dimension=0, tiled=True
    ).astype(jnp.float32)
    return (stream_own.astype(jnp.float32) + summed).astype(jnp.bfloat16)


MESH = pl.DeviceIdType.MESH


def layer_kernel(
    zn,
    table_ref,
    q_ref,
    lat_ref,
    key_ref,
    conv_ref,
    expand_hbm,
    res_hbm,
    out_w_hbm,
    gate_hbm,
    value_hbm,
    down_hbm,
    out_ref,
    expand_ref,
    res_ref,
    out_w_ref,
    gate_ref,
    value_ref,
    down_ref,
    lat_all,
    att_send,
    att_recv,
    nrm,
    stage,
    w_full,
    dn_full,
    hbuf,
    abuf,
    halo_send,
    halo_recv,
    part,
    c_send,
    c_recv,
    keep,
    x_send,
    x_recv,
    z_send,
    z_recv,
    in_s,
    lz_s, lz_r, ly_s, ly_r, lc_s, lc_r,
    wz_s, wz_r, wy_s, wy_r,
    dz_s, dz_r, dy_s, dy_r,
    at_s, at_r,
    nz_s, nz_r, nx_s, nx_r, nc_s, nc_r,
    h_s, h_r,
    pc_s, pc_r, px_s, px_r, pz_s, pz_r,
):
    f32, bf16 = jnp.float32, jnp.bfloat16
    s, t = lax.axis_index("sp"), lax.axis_index("tp")
    z, y = s // 2, s % 2
    x, c = t // 2, t % 2
    yo, xo, co = 1 - y, 1 - x, 1 - c
    rows = lat_ref.shape[0]
    half, share = rows // 2, rows // 4
    rank = lat_ref.shape[1]
    sub = down_ref.shape[0] // zn
    sp = 2 * zn

    def to_z(d):
        return {"sp": 2 * ((z + d) % zn) + y, "tp": t}

    y_dev = {"sp": 2 * z + yo, "tp": t}
    x_dev = {"sp": s, "tp": 2 * xo + c}
    c_dev = {"sp": s, "tp": 2 * x + co}

    def from_z(d):
        return (z + zn - d) % zn

    started = []

    def send(src, dst, s_sem, r_sem, dev):
        copy = pltpu.make_async_remote_copy(
            src_ref=src, dst_ref=dst, send_sem=s_sem, recv_sem=r_sem,
            device_id=dev, device_id_type=MESH,
        )
        copy.start()
        started.append(copy)
        return copy

    def arrived(dst, s_sem, r_sem):
        pltpu.make_async_remote_copy(
            src_ref=dst, dst_ref=dst, send_sem=s_sem, recv_sem=r_sem,
            device_id=c_dev, device_id_type=MESH,
        ).wait_recv()

    barrier = pltpu.get_barrier_semaphore()
    partners = [to_z(d) for d in range(1, zn)] + [y_dev, x_dev, c_dev, {"sp": s, "tp": 2 * xo + co}]
    for dev in partners:
        pl.semaphore_signal(barrier, inc=1, device_id=dev, device_id_type=MESH)

    mine_rows = pl.ds(pl.multiple_of(t * share, share), share)
    loads = [
        pltpu.make_async_copy(src, dst, in_s.at[i])
        for i, (src, dst) in enumerate(
            [
                (gate_hbm, gate_ref),
                (value_hbm, value_ref),
                (down_hbm, down_ref),
                (expand_hbm, expand_ref),
                (res_hbm.at[mine_rows, :], res_ref),
                (out_w_hbm, out_w_ref),
            ]
        )
    ]
    for load in loads:
        load.start()

    h = ROPE // 2
    cos, sine = table_ref[:h, :], table_ref[h:ROPE, :]

    def turn(v):
        a, b = v[:h], v[h:]
        return jnp.concatenate([a * cos - b * sine, b * cos + a * sine], axis=0)

    rot = NOPE_A + NOPE_B
    q = q_ref[...].astype(f32)
    pair = jnp.concatenate([turn(q[rot + ROPE :]), turn(key_ref[...].astype(f32))], axis=0).T.astype(bf16)
    q_narrow_t, key_turned = pair[:, :ROPE], pair[:, ROPE:]
    for i in range(2):
        lat_all[s, i, :, :rank] = lat_ref[i * half : (i + 1) * half, :]
        lat_all[s, i, :, rank : rank + ROPE] = key_turned[i * half : (i + 1) * half, :]
        lat_all[s, i, :, rank + ROPE :] = jnp.zeros((half, ROPE), bf16)
    pl.semaphore_wait(barrier, len(partners))

    mine = lat_all.at[s, c]
    for d in range(1, zn):
        send(mine, mine, lz_s.at[d], lz_r.at[d], to_z(d))
    send(mine, mine, ly_s.at[0], ly_r.at[0], y_dev)

    loads[0].wait()
    loads[1].wait()
    for k in range(zn):
        stage[k, :, :sub] = gate_ref[:, k * sub : (k + 1) * sub]
        stage[k, :, sub:] = value_ref[:, k * sub : (k + 1) * sub]
    for d in range(1, zn):
        send(stage.at[(z + d) % zn], w_full.at[s], wz_s.at[d], wz_r.at[d], to_z(d))
    w_full[s] = stage[z]
    loads[2].wait()

    def send_down(d):
        zz = (z + d) % zn
        piece = down_ref.at[pl.ds(pl.multiple_of(zz * sub, sub), sub), :]
        send(piece, dn_full.at[s], dz_s.at[d], dz_r.at[d], to_z(d))

    send_down(1)
    dn_full[s] = down_ref[pl.ds(pl.multiple_of(z * sub, sub), sub), :]

    for d in range(1, zn):
        blk = lat_all.at[2 * from_z(d) + y, c]
        arrived(blk, lz_s.at[d], lz_r.at[d])
        send(blk, blk, ly_s.at[d], ly_r.at[d], y_dev)
        send(blk, blk, lc_s.at[d], lc_r.at[d], c_dev)
    send(w_full.at[s], w_full.at[s], wy_s.at[0], wy_r.at[0], y_dev)
    for d in range(zn):
        blk = lat_all.at[2 * from_z(d) + yo, c]
        arrived(blk, ly_s.at[d], ly_r.at[d])
        send(blk, blk, lc_s.at[zn + d], lc_r.at[zn + d], c_dev)
    q_wide = q[:NOPE_A].T.astype(bf16)
    pair = jnp.concatenate([q[NOPE_A:rot], turn(q[rot : rot + ROPE])], axis=0).T.astype(bf16)
    q_narrow, q_wide_t = pair[:, :NOPE_B], pair[:, NOPE_B:]
    loads[3].wait()
    for d in range(1, zn):
        arrived(lat_all.at[2 * from_z(d) + y, co], lc_s.at[d], lc_r.at[d])
    for d in range(zn):
        arrived(lat_all.at[2 * from_z(d) + yo, co], lc_s.at[zn + d], lc_r.at[zn + d])

    whole = lat_all[...].reshape(sp * rows, lat_all.shape[3])
    expanded = jnp.dot(whole[:, :rank], expand_ref[...], preferred_element_type=f32).astype(bf16)
    keys_t = whole[:, rank : rank + ROPE]

    def attend(qc, qt, kc, v, scale):
        dims = (((1,), (1,)), ((), ()))
        scores = (
            lax.dot_general(qc, kc, dims, preferred_element_type=f32)
            + lax.dot_general(qt, keys_t, dims, preferred_element_type=f32)
        ) * scale
        w = jnp.exp(scores - jnp.max(scores, axis=1, keepdims=True))
        total = jnp.sum(w, axis=1, keepdims=True)
        return (jnp.dot(w.astype(bf16), v, preferred_element_type=f32) / total).astype(bf16)

    nb = NOPE_A + VAL_A
    wide = attend(q_wide, q_wide_t, expanded[:, :NOPE_A], expanded[:, NOPE_A:nb], (NOPE_A + ROPE) ** -0.5)
    narrow = attend(
        q_narrow, q_narrow_t, expanded[:, nb : nb + NOPE_B],
        expanded[:, nb + NOPE_B : nb + NOPE_B + VAL_B], (NOPE_B + ROPE) ** -0.5,
    )
    vals = VAL_A + VAL_B
    for i in range(4):
        att_send[i, :, :VAL_A] = wide[i * share : (i + 1) * share, :]
        att_send[i, :, VAL_A:vals] = narrow[i * share : (i + 1) * share, :]
    others = [(2 * x + co), (2 * xo + c), (2 * xo + co)]
    for i, o in enumerate(others):
        send(att_send.at[o], att_recv.at[t], at_s.at[i], at_r.at[i], {"sp": s, "tp": o})
    att_recv[t] = att_send[t]

    def forward(full, sz, rz, sy, ry, d):
        blk = full.at[2 * from_z(d) + y]
        arrived(blk, sz.at[d], rz.at[d])
        send(blk, blk, sy.at[d], ry.at[d], y_dev)

    def forward_weights(d):
        forward(w_full, wz_s, wz_r, wy_s, wy_r, d)

    loads[4].wait()
    loads[5].wait()
    for i, o in enumerate(others):
        arrived(att_recv.at[o], at_s.at[i], at_r.at[i])
    projected = jnp.dot(att_recv[0, :, :vals], out_w_ref[:vals, :], preferred_element_type=f32)
    for i in range(1, 4):
        projected += jnp.dot(
            att_recv[i, :, :vals], out_w_ref[i * vals : (i + 1) * vals, :], preferred_element_type=f32
        )
    stream = (res_ref[...].astype(f32) + projected).astype(bf16)
    stream_f = stream.astype(f32)
    scaled = stream_f * lax.rsqrt(jnp.mean(stream_f * stream_f, axis=1, keepdims=True) + 1e-06)
    for k in range(scaled.shape[1] // rows):
        gain = table_ref[ROPE + k : ROPE + k + 1, :]
        nrm[z, t, :, k * rows : (k + 1) * rows] = (scaled[:, k * rows : (k + 1) * rows] * gain).astype(bf16)

    own = nrm.at[z, t]
    for d in range(1, zn):
        send(own, own, nz_s.at[d], nz_r.at[d], to_z(d))
    send(own, own, nx_s.at[0], nx_r.at[0], x_dev)
    send(own, own, nc_s.at[0], nc_r.at[0], c_dev)
    for d in range(2, zn):
        send_down(d)
    forward_weights(1)
    xt = 2 * xo + c
    blk = nrm.at[z, xt]
    arrived(blk, nx_s.at[0], nx_r.at[0])
    send(blk, blk, nc_s.at[zn], nc_r.at[zn], c_dev)
    for d in range(1, zn):
        blk = nrm.at[from_z(d), t]
        arrived(blk, nz_s.at[d], nz_r.at[d])
        send(blk, blk, nx_s.at[d], nx_r.at[d], x_dev)
        send(blk, blk, nc_s.at[d], nc_r.at[d], c_dev)
        if d > 1:
            forward_weights(d)
    for d in range(1, zn):
        blk = nrm.at[from_z(d), xt]
        arrived(blk, nx_s.at[d], nx_r.at[d])
        send(blk, blk, nc_s.at[zn + d], nc_r.at[zn + d], c_dev)
    send(dn_full.at[s], dn_full.at[s], dy_s.at[0], dy_r.at[0], y_dev)
    forward(dn_full, dz_s, dz_r, dy_s, dy_r, 1)
    for d in range(zn):
        arrived(w_full.at[2 * from_z(d) + yo], wy_s.at[d], wy_r.at[d])
    weights = w_full[...].reshape(sp * w_full.shape[1], 2 * sub)
    for d in range(zn):
        zz = from_z(d)
        arrived(nrm.at[zz, 2 * x + co], nc_s.at[d], nc_r.at[d])
        arrived(nrm.at[zz, 2 * xo + co], nc_s.at[zn + d], nc_r.at[zn + d])
        block = nrm[zz].reshape(rows, nrm.shape[3])
        hbuf[zz] = jnp.dot(block, weights, preferred_element_type=f32).astype(bf16)

    wide_lanes = halo_send.shape[1]
    for k in range(zn):
        g = hbuf[k, :, :wide_lanes].astype(f32)
        halo_send[k : k + 1, :] = g[rows - 1 : rows, :]
        halo_send[zn + k : zn + k + 1, :] = g[0:1, :]
    send(halo_send, halo_recv, h_s.at[0], h_r.at[0], y_dev)
    for d in range(2, zn):
        forward(dn_full, dz_s, dz_r, dy_s, dy_r, d)
    taps = jnp.zeros((conv_ref.shape[0], wide_lanes), f32)
    conv_all = conv_ref[...].astype(f32)
    pieces = [conv_all[:, k * sub : (k + 1) * sub] for k in range(zn)]
    taps = pieces[0]
    for k in range(1, zn):
        taps = jnp.where(z == k, pieces[k], taps)
    taps = jnp.concatenate([taps, jnp.zeros((taps.shape[0], wide_lanes - sub), f32)], axis=1)
    row_id = lax.broadcasted_iota(jnp.int32, (rows, wide_lanes), 0)
    arrived(halo_recv, h_s.at[0], h_r.at[0])
    nothing = jnp.zeros((1, wide_lanes), f32)
    for k in range(zn):
        before_low = halo_recv[k - 1 : k, :] if k > 0 else nothing
        before = jnp.where(y == 0, before_low, halo_recv[k : k + 1, :])
        after_high = halo_recv[zn + k + 1 : zn + k + 2, :] if k < zn - 1 else nothing
        after = jnp.where(y == 0, halo_recv[zn + k : zn + k + 1, :], after_high)
        g = hbuf[k, :, :wide_lanes].astype(f32)
        up = jnp.where(row_id == 0, before, pltpu.roll(g, 1, 0))
        down = jnp.where(row_id == rows - 1, after, pltpu.roll(g, rows - 1, 0))
        mixed = up * taps[0:1] + g * taps[1:2] + down * taps[2:3]
        mixed = mixed[:, :sub]
        v = hbuf[k].astype(f32)[:, sub:]
        abuf[k] = (mixed / (1.0 + jnp.exp(-mixed)) * v).astype(bf16)

    for d in range(zn):
        arrived(dn_full.at[2 * from_z(d) + yo], dy_s.at[d], dy_r.at[d])
    order = list(range(1, zn)) + [0]
    depth = dn_full.shape[2]
    for d in order:
        zz = (z + d) % zn
        a = abuf[zz]
        for k in range(sp):
            p = jnp.dot(a, dn_full[k], preferred_element_type=f32)
            part[d, :, :, k * depth : (k + 1) * depth] = p.reshape(4, share, depth)
        for i in range(2):
            c_send[d, i] = part[d, 2 * i + co].astype(bf16)
        send(c_send.at[d], c_recv.at[d], pc_s.at[d], pc_r.at[d], c_dev)
    for d in order:
        arrived(c_recv.at[d], pc_s.at[d], pc_r.at[d])
        x_send[d] = (part[d, 2 * xo + c] + c_recv[d, xo].astype(f32)).astype(bf16)
        send(x_send.at[d], x_recv.at[d], px_s.at[d], px_r.at[d], x_dev)
        keep[d] = part[d, 2 * x + c] + c_recv[d, x].astype(f32)
    for d in order:
        arrived(x_recv.at[d], px_s.at[d], px_r.at[d])
        if d > 0:
            z_send[d] = (keep[d] + x_recv[d].astype(f32)).astype(bf16)
            send(z_send.at[d], z_recv.at[d], pz_s.at[d], pz_r.at[d], to_z(d))
    total = keep[0] + x_recv[0].astype(f32)
    for d in range(1, zn):
        arrived(z_recv.at[d], pz_s.at[d], pz_r.at[d])
        total += z_recv[d].astype(f32)
    out_ref[...] = (stream_f + total).astype(bf16)
    for copy in started:
        copy.wait_send()


def kernel_body(zn, *args):
    (queries, latents, shared_key, expand_weight, residual, out_weight, norm_gain,
     gate_weight, value_weight, conv_weight, down_weight) = args
    rows, width = residual.shape
    sub = down_weight.shape[0] // zn
    share, half = rows // 4, rows // 2
    d_own = gate_weight.shape[0]
    positions = lax.axis_index("sp") * rows + jnp.arange(rows, dtype=jnp.int32)
    cos_table, sine_table = tables(positions, ROPE)
    gain = norm_gain.reshape(width // rows, rows).astype(jnp.float32)
    table = jnp.concatenate([cos_table.T, sine_table.T, gain], axis=0)
    bf16, f32 = jnp.bfloat16, jnp.float32
    vals = VAL_A + VAL_B
    lanes = -(-vals // 128) * 128
    halo_lanes = -(-sub // 128) * 128
    V, DMA = pltpu.VMEM, pltpu.SemaphoreType.DMA
    sems = [DMA((6,))]
    for count in (zn, zn, 2 * zn, zn, zn, zn, zn, 3, zn, zn, 2 * zn, 1, zn, zn, zn):
        sems += [DMA((count,)), DMA((count,))]
    return pl.pallas_call(
        functools.partial(layer_kernel, zn),
        out_shape=jax.ShapeDtypeStruct((share, width), bf16),
        in_specs=[pl.BlockSpec(memory_space=V)] * 5 + [pl.BlockSpec(memory_space=pl.ANY)] * 6,
        out_specs=pl.BlockSpec(memory_space=V),
        scratch_shapes=[
            V(expand_weight.shape, bf16),
            V((share, width), bf16),
            V(out_weight.shape, bf16),
            V(gate_weight.shape, bf16),
            V(value_weight.shape, bf16),
            V(down_weight.shape, bf16),
            V((2 * zn, 2, half, latents.shape[1] + 2 * ROPE), bf16),
            V((4, share, lanes), bf16),
            V((4, share, lanes), bf16),
            V((zn, 4, share, width), bf16),
            V((zn, d_own, 2 * sub), bf16),
            V((2 * zn, d_own, 2 * sub), bf16),
            V((2 * zn, sub, down_weight.shape[1]), bf16),
            V((zn, rows, 2 * sub), bf16),
            V((zn, rows, sub), bf16),
            V((2 * zn, halo_lanes), f32),
            V((2 * zn, halo_lanes), f32),
            V((zn, 4, share, width), f32),
            V((zn, 2, share, width), bf16),
            V((zn, 2, share, width), bf16),
            V((zn, share, width), f32),
            V((zn, share, width), bf16),
            V((zn, share, width), bf16),
            V((zn, share, width), bf16),
            V((zn, share, width), bf16),
        ] + sems,
        compiler_params=pltpu.CompilerParams(collective_id=0, has_side_effects=True),
    )(table, queries.T, latents, shared_key.T, conv_weight, expand_weight, residual, out_weight,
      gate_weight, value_weight, down_weight)


def pick(*args):
    zn = lax.axis_size("sp") // 2
    hidden = args[10].shape[0]
    sub = hidden // zn
    fits = (
        lax.axis_size("sp") % 2 == 0
        and lax.axis_size("tp") == 4
        and hidden % zn == 0
        and sub % 64 == 0
        and args[7].shape[0] % 128 == 0
        and args[0].shape[0] % 128 == 0
        and args[4].shape[1] % args[0].shape[0] == 0
        and args[9].shape[0] == 3
    )
    return kernel_body(zn, *args) if fits else body(*args)


def solution(mesh):
    in_specs = (
        P("sp", "tp"),
        P("sp", None),
        P("sp", None),
        P(None, "tp"),
        P("sp", None),
        P(),
        P(),
        P("sp", "tp"),
        P("sp", "tp"),
        P(None, "tp"),
        P("tp", "sp"),
    )
    out_specs = P(("sp", "tp"), None)
    return jax.shard_map(pick, mesh=mesh, in_specs=in_specs, out_specs=out_specs, check_vma=False)
```

profile of v0, /device:TPU:0, one launch (start us, length us, event | category | flops | bytes accessed | tf_op | source)
XLA Modules:
  0.0 91.3 jit_solution(4614274909899172051)
XLA Ops:
  0.0 0.7 bitcast_convert_fusion
  0.7 0.1 multiply_cosine_fusion
  0.9 0.6 pad_maximum_fusion.table_ref
  1.5 88.2 %shard_map.109 = bf16[32,2048]{1,0:T(8,128)(2,1)} custom-call(f32[80,128]{1,0:T(8,128)} %pad_maximum_fusion.table_ref, bf16[320,128]{1,0:T(8,128)(2,1)} %bitcast.5, bf16[128,512]{1,0:T(8,128)(2,1)} %lat_ref.1, bf16[64,128]{1,0:T(8,128)(2,1)} %bitcast.6, bf16[3,768]{1,0:T(4,128)(2,1)} %conv_ref.1, bf16[512,384]{1,0:T(8,128)(2,1)} %expand_hbm.1, ...), custom_call_target="tpu_custom_call" | custom-call | tf_op jit(solution)/shard_map/pallas_call | solution.py:534
  89.7 1.6 %copy.13 = bf16[32,2048]{1,0:T(8,128)(2,1)} copy(bf16[32,2048]{1,0:T(8,128)(2,1)} %shard_map.109) | data formatting | bytes 262144
  (2 shorter events, 0.0 us)
where the time goes:
time: 91.4 us; the launch traced here: 91.3 us
  Pallas kernels  88.2 us (96%)
  local copies, waits for them, and re-layouts  1.57 us (2%)
  other arithmetic  1.47 us (2%)
    pallas_call x1, Pallas kernels, kernel_body(): pl.pallas_call(functools.partial(layer_kernel, zn), out_shape=jax.ShapeDt...  88.2 us

commit v1 on v0

--- a/solution.py
+++ b/solution.py
@@ -1,4 +1,5 @@
 import functools
+import math
 
 import jax
 import jax.numpy as jnp
@@ -192,15 +193,20 @@
 
 
 MESH = pl.DeviceIdType.MESH
+KINDS = (
+    "lz", "ly", "lx", "lxy", "lcz", "lcx", "lcy", "lcxy",
+    "wz", "wy", "dz", "dy", "nz", "nx", "ncz", "ncx", "at", "pc", "px", "pz", "h",
+)
+SENDS = 96
 
 
 def layer_kernel(
     zn,
-    table_ref,
-    q_ref,
-    lat_ref,
-    key_ref,
-    conv_ref,
+    q_hbm,
+    lat_hbm,
+    key_hbm,
+    conv_hbm,
+    gain_hbm,
     expand_hbm,
     res_hbm,
     out_w_hbm,
@@ -208,6 +214,11 @@
     value_hbm,
     down_hbm,
     out_ref,
+    q_ref,
+    lat_ref,
+    key_ref,
+    conv_ref,
+    gain_ref,
     expand_ref,
     res_ref,
     out_w_ref,
@@ -217,6 +228,7 @@
     lat_all,
     att_send,
     att_recv,
+    own_stream,
     nrm,
     stage,
     w_full,
@@ -234,142 +246,186 @@
     z_send,
     z_recv,
     in_s,
-    lz_s, lz_r, ly_s, ly_r, lc_s, lc_r,
-    wz_s, wz_r, wy_s, wy_r,
-    dz_s, dz_r, dy_s, dy_r,
-    at_s, at_r,
-    nz_s, nz_r, nx_s, nx_r, nc_s, nc_r,
-    h_s, h_r,
-    pc_s, pc_r, px_s, px_r, pz_s, pz_r,
+    send_s,
+    recv_s,
 ):
     f32, bf16 = jnp.float32, jnp.bfloat16
     s, t = lax.axis_index("sp"), lax.axis_index("tp")
     z, y = s // 2, s % 2
     x, c = t // 2, t % 2
     yo, xo, co = 1 - y, 1 - x, 1 - c
+    xt, ct, xct = 2 * xo + c, 2 * x + co, 2 * xo + co
     rows = lat_ref.shape[0]
-    half, share = rows // 2, rows // 4
+    share = rows // 4
+    packed = share // 2
     rank = lat_ref.shape[1]
     sub = down_ref.shape[0] // zn
     sp = 2 * zn
 
-    def to_z(d):
-        return {"sp": 2 * ((z + d) % zn) + y, "tp": t}
+    inner = ((z + 1) // 2) % 2
+    near = z + 1 - 2 * (z % 2)
+    mid = (z + 2) % zn + inner * (zn - 1 - z - (z + 2) % zn)
+    far = zn - 1 - z + inner * ((z + 2) % zn - (zn - 1 - z))
+    arrivals = (near + inner * (mid - near), mid + inner * (far - mid), far + inner * (near - far))
+
+    def to_z(zz):
+        return {"sp": 2 * zz + y, "tp": t}
 
     y_dev = {"sp": 2 * z + yo, "tp": t}
-    x_dev = {"sp": s, "tp": 2 * xo + c}
-    c_dev = {"sp": s, "tp": 2 * x + co}
-
-    def from_z(d):
-        return (z + zn - d) % zn
+    x_dev = {"sp": s, "tp": xt}
+    c_dev = {"sp": s, "tp": ct}
+    xc_dev = {"sp": s, "tp": xct}
 
     started = []
-
-    def send(src, dst, s_sem, r_sem, dev):
-        copy = pltpu.make_async_remote_copy(
-            src_ref=src, dst_ref=dst, send_sem=s_sem, recv_sem=r_sem,
-            device_id=dev, device_id_type=MESH,
+    used = [0]
+
+    def copy_to(src, dst, dev, kind, i, slot):
+        return pltpu.make_async_remote_copy(
+            src_ref=src, dst_ref=dst, send_sem=send_s.at[slot],
+            recv_sem=recv_s.at[KINDS.index(kind) * zn + i], device_id=dev, device_id_type=MESH,
         )
+
+    def new_slot():
+        used[0] += 1
+        return used[0] - 1
+
+    def send(ref, dev, kind, i, dst=None):
+        copy = copy_to(ref, ref if dst is None else dst, dev, kind, i, new_slot())
         copy.start()
         started.append(copy)
-        return copy
-
-    def arrived(dst, s_sem, r_sem):
-        pltpu.make_async_remote_copy(
-            src_ref=dst, dst_ref=dst, send_sem=s_sem, recv_sem=r_sem,
-            device_id=c_dev, device_id_type=MESH,
-        ).wait_recv()
+
+    def arrived(dst, kind, i):
+        with jax.named_scope("wait_" + kind):
+            copy_to(dst, dst, c_dev, kind, i, 0).wait_recv()
 
     barrier = pltpu.get_barrier_semaphore()
-    partners = [to_z(d) for d in range(1, zn)] + [y_dev, x_dev, c_dev, {"sp": s, "tp": 2 * xo + co}]
+    partners = [to_z(near), to_z(mid), to_z(far), y_dev, x_dev, c_dev, xc_dev]
     for dev in partners:
         pl.semaphore_signal(barrier, inc=1, device_id=dev, device_id_type=MESH)
 
-    mine_rows = pl.ds(pl.multiple_of(t * share, share), share)
-    loads = [
-        pltpu.make_async_copy(src, dst, in_s.at[i])
-        for i, (src, dst) in enumerate(
-            [
-                (gate_hbm, gate_ref),
-                (value_hbm, value_ref),
-                (down_hbm, down_ref),
-                (expand_hbm, expand_ref),
-                (res_hbm.at[mine_rows, :], res_ref),
-                (out_w_hbm, out_w_ref),
-            ]
-        )
+    def res_rows(i):
+        return res_hbm.at[pl.ds(pl.multiple_of((2 * i + c) * share, share), share), :]
+
+    pairs = [
+        (key_hbm, key_ref),
+        (lat_hbm, lat_ref),
+        (gate_hbm, gate_ref),
+        (value_hbm, value_ref),
+        (q_hbm, q_ref),
+        (down_hbm, down_ref),
+        (expand_hbm, expand_ref),
+        (res_rows(0), res_ref.at[0]),
+        (res_rows(1), res_ref.at[1]),
+        (gain_hbm, gain_ref),
+        (conv_hbm, conv_ref),
+        (out_w_hbm, out_w_ref),
     ]
+    loads = [pltpu.make_async_copy(src, dst, in_s.at[i]) for i, (src, dst) in enumerate(pairs)]
     for load in loads:
         load.start()
 
     h = ROPE // 2
-    cos, sine = table_ref[:h, :], table_ref[h:ROPE, :]
+    step = lax.broadcasted_iota(jnp.int32, (h, rows), 0).astype(f32) * (-math.log(10000.0) / h)
+    spot = (s * rows + lax.broadcasted_iota(jnp.int32, (h, rows), 1)).astype(f32)
+    angles = spot * jnp.exp(step)
+    cos, sine = jnp.cos(angles), jnp.sin(angles)
 
     def turn(v):
         a, b = v[:h], v[h:]
         return jnp.concatenate([a * cos - b * sine, b * cos + a * sine], axis=0)
 
-    rot = NOPE_A + NOPE_B
-    q = q_ref[...].astype(f32)
-    pair = jnp.concatenate([turn(q[rot + ROPE :]), turn(key_ref[...].astype(f32))], axis=0).T.astype(bf16)
-    q_narrow_t, key_turned = pair[:, :ROPE], pair[:, ROPE:]
-    for i in range(2):
-        lat_all[s, i, :, :rank] = lat_ref[i * half : (i + 1) * half, :]
-        lat_all[s, i, :, rank : rank + ROPE] = key_turned[i * half : (i + 1) * half, :]
-        lat_all[s, i, :, rank + ROPE :] = jnp.zeros((half, ROPE), bf16)
-    pl.semaphore_wait(barrier, len(partners))
-
-    mine = lat_all.at[s, c]
-    for d in range(1, zn):
-        send(mine, mine, lz_s.at[d], lz_r.at[d], to_z(d))
-    send(mine, mine, ly_s.at[0], ly_r.at[0], y_dev)
-
     loads[0].wait()
+    turned = turn(key_ref[...].astype(f32))
+    key_turned = jnp.concatenate([turned, jnp.zeros_like(turned)], axis=0).T.astype(bf16)[:, :ROPE]
     loads[1].wait()
+    for i in range(4):
+        for j in range(2):
+            first = i * share + j * packed
+            lat_all[s, i, :, j * rank : (j + 1) * rank] = lat_ref[first : first + packed, :]
+        lat_all[s, i, :, 2 * rank :] = jnp.concatenate(
+            [key_turned[i * share : i * share + packed], key_turned[i * share + packed : (i + 1) * share]], axis=1
+        )
+    loads[2].wait()
+    loads[3].wait()
     for k in range(zn):
         stage[k, :, :sub] = gate_ref[:, k * sub : (k + 1) * sub]
         stage[k, :, sub:] = value_ref[:, k * sub : (k + 1) * sub]
-    for d in range(1, zn):
-        send(stage.at[(z + d) % zn], w_full.at[s], wz_s.at[d], wz_r.at[d], to_z(d))
+    with jax.named_scope("barrier"):
+        pl.semaphore_wait(barrier, len(partners))
+
+    def lat(zz, yy, q):
+        return lat_all.at[2 * zz + yy, q]
+
+    for zz in (far, mid, near):
+        send(lat(z, y, t), to_z(zz), "lz", z)
+    send(lat(z, y, t), y_dev, "ly", z)
+    send(lat(z, y, xt), y_dev, "lxy", z)
+    for zz in (far, mid, near):
+        send(stage.at[zz], to_z(zz), "wz", z, w_full.at[s])
     w_full[s] = stage[z]
-    loads[2].wait()
-
-    def send_down(d):
-        zz = (z + d) % zn
-        piece = down_ref.at[pl.ds(pl.multiple_of(zz * sub, sub), sub), :]
-        send(piece, dn_full.at[s], dz_s.at[d], dz_r.at[d], to_z(d))
-
-    send_down(1)
-    dn_full[s] = down_ref[pl.ds(pl.multiple_of(z * sub, sub), sub), :]
-
-    for d in range(1, zn):
-        blk = lat_all.at[2 * from_z(d) + y, c]
-        arrived(blk, lz_s.at[d], lz_r.at[d])
-        send(blk, blk, ly_s.at[d], ly_r.at[d], y_dev)
-        send(blk, blk, lc_s.at[d], lc_r.at[d], c_dev)
-    send(w_full.at[s], w_full.at[s], wy_s.at[0], wy_r.at[0], y_dev)
-    for d in range(zn):
-        blk = lat_all.at[2 * from_z(d) + yo, c]
-        arrived(blk, ly_s.at[d], ly_r.at[d])
-        send(blk, blk, lc_s.at[zn + d], lc_r.at[zn + d], c_dev)
+
+    for zz in arrivals:
+        arrived(lat(zz, y, t), "lz", zz)
+        send(lat(zz, y, t), y_dev, "ly", zz)
+        send(lat(zz, y, t), x_dev, "lx", zz)
+        send(lat(zz, y, t), c_dev, "lcz", zz)
+    send(w_full.at[s], y_dev, "wy", z)
+    arrived(lat(z, yo, t), "ly", z)
+    send(lat(z, yo, t), c_dev, "lcy", z)
+    arrived(lat(z, yo, xt), "lxy", z)
+    send(lat(z, yo, xt), c_dev, "lcxy", z)
+    for i, zz in enumerate(arrivals):
+        arrived(lat(zz, yo, t), "ly", zz)
+        if i < 2:
+            send(lat(zz, yo, t), x_dev, "lxy", zz)
+        send(lat(zz, yo, t), c_dev, "lcy", zz)
+        arrived(lat(zz, y, xt), "lx", zz)
+        if i == 2:
+            send(lat(zz, y, xt), y_dev, "lxy", zz)
+        send(lat(zz, y, xt), c_dev, "lcx", zz)
+
+    loads[4].wait()
+    rot = NOPE_A + NOPE_B
+    q = q_ref[...].astype(f32)
     q_wide = q[:NOPE_A].T.astype(bf16)
     pair = jnp.concatenate([q[NOPE_A:rot], turn(q[rot : rot + ROPE])], axis=0).T.astype(bf16)
     q_narrow, q_wide_t = pair[:, :NOPE_B], pair[:, NOPE_B:]
-    loads[3].wait()
-    for d in range(1, zn):
-        arrived(lat_all.at[2 * from_z(d) + y, co], lc_s.at[d], lc_r.at[d])
-    for d in range(zn):
-        arrived(lat_all.at[2 * from_z(d) + yo, co], lc_s.at[zn + d], lc_r.at[zn + d])
-
-    whole = lat_all[...].reshape(sp * rows, lat_all.shape[3])
-    expanded = jnp.dot(whole[:, :rank], expand_ref[...], preferred_element_type=f32).astype(bf16)
-    keys_t = whole[:, rank : rank + ROPE]
+    turned = turn(q[rot + ROPE :])
+    q_narrow_t = jnp.concatenate([turned, jnp.zeros_like(turned)], axis=0).T.astype(bf16)[:, :ROPE]
+    loads[5].wait()
+    dn_full[s] = down_ref[pl.ds(pl.multiple_of(z * sub, sub), sub), :]
+    loads[6].wait()
+
+    for zz in arrivals:
+        arrived(lat(zz, yo, xt), "lxy", zz)
+        send(lat(zz, yo, xt), c_dev, "lcxy", zz)
+    for zz in arrivals:
+        arrived(lat(zz, y, ct), "lcz", zz)
+        arrived(lat(zz, y, xct), "lcx", zz)
+    for zz in (z,) + arrivals:
+        arrived(lat(zz, yo, ct), "lcy", zz)
+        arrived(lat(zz, yo, xct), "lcxy", zz)
+
+    whole = lat_all[...].reshape(sp * 4 * packed, lat_all.shape[3])
+    expand_w = expand_ref[...]
+    expanded = jnp.concatenate(
+        [
+            jnp.dot(whole[:, j * rank : (j + 1) * rank], expand_w, preferred_element_type=f32).astype(bf16)
+            for j in range(2)
+        ],
+        axis=0,
+    )
+    keys_t = whole[:, 2 * rank :]
+    empty = jnp.zeros((rows, ROPE), bf16)
 
     def attend(qc, qt, kc, v, scale):
         dims = (((1,), (1,)), ((), ()))
+        turned_scores = [
+            lax.dot_general(jnp.concatenate(two, axis=1), keys_t, dims, preferred_element_type=f32)
+            for two in ([qt, empty], [empty, qt])
+        ]
         scores = (
-            lax.dot_general(qc, kc, dims, preferred_element_type=f32)
-            + lax.dot_general(qt, keys_t, dims, preferred_element_type=f32)
+            lax.dot_general(qc, kc, dims, preferred_element_type=f32) + jnp.concatenate(turned_scores, axis=1)
         ) * scale
         w = jnp.exp(scores - jnp.max(scores, axis=1, keepdims=True))
         total = jnp.sum(w, axis=1, keepdims=True)
@@ -383,69 +439,79 @@
     )
     vals = VAL_A + VAL_B
     for i in range(4):
-        att_send[i, :, :VAL_A] = wide[i * share : (i + 1) * share, :]
-        att_send[i, :, VAL_A:vals] = narrow[i * share : (i + 1) * share, :]
-    others = [(2 * x + co), (2 * xo + c), (2 * xo + co)]
-    for i, o in enumerate(others):
-        send(att_send.at[o], att_recv.at[t], at_s.at[i], at_r.at[i], {"sp": s, "tp": o})
-    att_recv[t] = att_send[t]
-
-    def forward(full, sz, rz, sy, ry, d):
-        blk = full.at[2 * from_z(d) + y]
-        arrived(blk, sz.at[d], rz.at[d])
-        send(blk, blk, sy.at[d], ry.at[d], y_dev)
-
-    def forward_weights(d):
-        forward(w_full, wz_s, wz_r, wy_s, wy_r, d)
-
-    loads[4].wait()
-    loads[5].wait()
-    for i, o in enumerate(others):
-        arrived(att_recv.at[o], at_s.at[i], at_r.at[i])
-    projected = jnp.dot(att_recv[0, :, :vals], out_w_ref[:vals, :], preferred_element_type=f32)
-    for i in range(1, 4):
-        projected += jnp.dot(
-            att_recv[i, :, :vals], out_w_ref[i * vals : (i + 1) * vals, :], preferred_element_type=f32
+        att_send[i % 2, i // 2, :, :VAL_A] = wide[i * share : (i + 1) * share, :]
+        att_send[i % 2, i // 2, :, VAL_A:vals] = narrow[i * share : (i + 1) * share, :]
+    send(att_send.at[c], x_dev, "at", t, att_recv.at[t])
+    send(att_send.at[co], xc_dev, "at", t, att_recv.at[t])
+    send(att_send.at[co], c_dev, "at", t, att_recv.at[t])
+    att_recv[t] = att_send[c]
+
+    def forward_weights(zz):
+        arrived(w_full.at[2 * zz + y], "wz", zz)
+        send(w_full.at[2 * zz + y], y_dev, "wy", zz)
+
+    for load in loads[7:]:
+        load.wait()
+    forward_weights(arrivals[0])
+    for o in (ct, xt, xct):
+        arrived(att_recv.at[o], "at", o)
+
+    projected = None
+    for i in range(4):
+        term = jnp.dot(
+            att_recv[i].reshape(2 * share, att_recv.shape[3])[:, :vals],
+            out_w_ref[i * vals : (i + 1) * vals, :], preferred_element_type=f32,
         )
-    stream = (res_ref[...].astype(f32) + projected).astype(bf16)
+        projected = term if projected is None else projected + term
+    stream = (res_ref[...].reshape(2 * share, res_ref.shape[2]).astype(f32) + projected).astype(bf16)
     stream_f = stream.astype(f32)
     scaled = stream_f * lax.rsqrt(jnp.mean(stream_f * stream_f, axis=1, keepdims=True) + 1e-06)
-    for k in range(scaled.shape[1] // rows):
-        gain = table_ref[ROPE + k : ROPE + k + 1, :]
-        nrm[z, t, :, k * rows : (k + 1) * rows] = (scaled[:, k * rows : (k + 1) * rows] * gain).astype(bf16)
+    normed = (scaled * gain_ref[...].astype(f32)).astype(bf16)
+    for i in range(2):
+        nrm[z, 2 * i + c] = normed[i * share : (i + 1) * share]
+        own_stream[i] = stream[i * share : (i + 1) * share]
 
     own = nrm.at[z, t]
-    for d in range(1, zn):
-        send(own, own, nz_s.at[d], nz_r.at[d], to_z(d))
-    send(own, own, nx_s.at[0], nx_r.at[0], x_dev)
-    send(own, own, nc_s.at[0], nc_r.at[0], c_dev)
-    for d in range(2, zn):
-        send_down(d)
-    forward_weights(1)
-    xt = 2 * xo + c
-    blk = nrm.at[z, xt]
-    arrived(blk, nx_s.at[0], nx_r.at[0])
-    send(blk, blk, nc_s.at[zn], nc_r.at[zn], c_dev)
-    for d in range(1, zn):
-        blk = nrm.at[from_z(d), t]
-        arrived(blk, nz_s.at[d], nz_r.at[d])
-        send(blk, blk, nx_s.at[d], nx_r.at[d], x_dev)
-        send(blk, blk, nc_s.at[d], nc_r.at[d], c_dev)
-        if d > 1:
-            forward_weights(d)
-    for d in range(1, zn):
-        blk = nrm.at[from_z(d), xt]
-        arrived(blk, nx_s.at[d], nx_r.at[d])
-        send(blk, blk, nc_s.at[zn + d], nc_r.at[zn + d], c_dev)
-    send(dn_full.at[s], dn_full.at[s], dy_s.at[0], dy_r.at[0], y_dev)
-    forward(dn_full, dz_s, dz_r, dy_s, dy_r, 1)
-    for d in range(zn):
-        arrived(w_full.at[2 * from_z(d) + yo], wy_s.at[d], wy_r.at[d])
+    send(own, to_z(mid), "nz", z)
+    send(own, to_z(near), "nz", z)
+    send(own, c_dev, "ncz", z)
+    send(nrm.at[z, xt], c_dev, "ncx", z)
+
+    def send_down(zz):
+        piece = down_ref.at[pl.ds(pl.multiple_of(zz * sub, sub), sub), :]
+        send(piece, to_z(zz), "dz", z, dn_full.at[s])
+
+    send_down(far)
+    send_down(mid)
+    forward_weights(arrivals[1])
+    passed = []
+    for i, zz in enumerate(arrivals):
+        blk = nrm.at[zz, t]
+        arrived(blk, "nz", zz)
+        if i < 2:
+            on = copy_to(blk, blk, to_z(near), "nz", zz, new_slot())
+            passed.append(on)
+
+            @pl.when(inner == 1)
+            def _():
+                on.start()
+
+        send(blk, x_dev, "nx", zz)
+        send(blk, c_dev, "ncz", zz)
+        if i == 0:
+            forward_weights(arrivals[2])
+    send_down(near)
+    send(dn_full.at[s], y_dev, "dy", z)
+    for zz in (z,) + arrivals:
+        arrived(w_full.at[2 * zz + yo], "wy", zz)
     weights = w_full[...].reshape(sp * w_full.shape[1], 2 * sub)
-    for d in range(zn):
-        zz = from_z(d)
-        arrived(nrm.at[zz, 2 * x + co], nc_s.at[d], nc_r.at[d])
-        arrived(nrm.at[zz, 2 * xo + co], nc_s.at[zn + d], nc_r.at[zn + d])
+    for i, zz in enumerate((z,) + arrivals):
+        if i > 0:
+            blk = nrm.at[zz, xt]
+            arrived(blk, "nx", zz)
+            send(blk, c_dev, "ncx", zz)
+        arrived(nrm.at[zz, ct], "ncz", zz)
+        arrived(nrm.at[zz, xct], "ncx", zz)
         block = nrm[zz].reshape(rows, nrm.shape[3])
         hbuf[zz] = jnp.dot(block, weights, preferred_element_type=f32).astype(bf16)
 
@@ -454,10 +520,14 @@
         g = hbuf[k, :, :wide_lanes].astype(f32)
         halo_send[k : k + 1, :] = g[rows - 1 : rows, :]
         halo_send[zn + k : zn + k + 1, :] = g[0:1, :]
-    send(halo_send, halo_recv, h_s.at[0], h_r.at[0], y_dev)
-    for d in range(2, zn):
-        forward(dn_full, dz_s, dz_r, dy_s, dy_r, d)
-    taps = jnp.zeros((conv_ref.shape[0], wide_lanes), f32)
+    send(halo_send, y_dev, "h", 0, halo_recv)
+
+    def forward_down(zz):
+        arrived(dn_full.at[2 * zz + y], "dz", zz)
+        send(dn_full.at[2 * zz + y], y_dev, "dy", zz)
+
+    for zz in arrivals:
+        forward_down(zz)
     conv_all = conv_ref[...].astype(f32)
     pieces = [conv_all[:, k * sub : (k + 1) * sub] for k in range(zn)]
     taps = pieces[0]
@@ -465,7 +535,7 @@
         taps = jnp.where(z == k, pieces[k], taps)
     taps = jnp.concatenate([taps, jnp.zeros((taps.shape[0], wide_lanes - sub), f32)], axis=1)
     row_id = lax.broadcasted_iota(jnp.int32, (rows, wide_lanes), 0)
-    arrived(halo_recv, h_s.at[0], h_r.at[0])
+    arrived(halo_recv, "h", 0)
     nothing = jnp.zeros((1, wide_lanes), f32)
     for k in range(zn):
         before_low = halo_recv[k - 1 : k, :] if k > 0 else nothing
@@ -480,36 +550,42 @@
         v = hbuf[k].astype(f32)[:, sub:]
         abuf[k] = (mixed / (1.0 + jnp.exp(-mixed)) * v).astype(bf16)
 
-    for d in range(zn):
-        arrived(dn_full.at[2 * from_z(d) + yo], dy_s.at[d], dy_r.at[d])
-    order = list(range(1, zn)) + [0]
+    for zz in (z,) + arrivals:
+        arrived(dn_full.at[2 * zz + yo], "dy", zz)
+    order = (far, mid, near, z)
     depth = dn_full.shape[2]
-    for d in order:
-        zz = (z + d) % zn
+    for d, zz in enumerate(order):
         a = abuf[zz]
         for k in range(sp):
             p = jnp.dot(a, dn_full[k], preferred_element_type=f32)
             part[d, :, :, k * depth : (k + 1) * depth] = p.reshape(4, share, depth)
         for i in range(2):
             c_send[d, i] = part[d, 2 * i + co].astype(bf16)
-        send(c_send.at[d], c_recv.at[d], pc_s.at[d], pc_r.at[d], c_dev)
-    for d in order:
-        arrived(c_recv.at[d], pc_s.at[d], pc_r.at[d])
-        x_send[d] = (part[d, 2 * xo + c] + c_recv[d, xo].astype(f32)).astype(bf16)
-        send(x_send.at[d], x_recv.at[d], px_s.at[d], px_r.at[d], x_dev)
-        keep[d] = part[d, 2 * x + c] + c_recv[d, x].astype(f32)
-    for d in order:
-        arrived(x_recv.at[d], px_s.at[d], px_r.at[d])
-        if d > 0:
+        send(c_send.at[d], c_dev, "pc", d, c_recv.at[d])
+    for d, zz in enumerate(order):
+        arrived(c_recv.at[d], "pc", d)
+        x_send[d] = (part[d, xt] + c_recv[d, xo].astype(f32)).astype(bf16)
+        send(x_send.at[d], x_dev, "px", d, x_recv.at[d])
+        keep[d] = part[d, t] + c_recv[d, x].astype(f32)
+    total = own_stream[x].astype(f32)
+    for d, zz in enumerate(order):
+        arrived(x_recv.at[d], "px", d)
+        if d < zn - 1:
             z_send[d] = (keep[d] + x_recv[d].astype(f32)).astype(bf16)
-            send(z_send.at[d], z_recv.at[d], pz_s.at[d], pz_r.at[d], to_z(d))
-    total = keep[0] + x_recv[0].astype(f32)
-    for d in range(1, zn):
-        arrived(z_recv.at[d], pz_s.at[d], pz_r.at[d])
-        total += z_recv[d].astype(f32)
-    out_ref[...] = (stream_f + total).astype(bf16)
+            send(z_send.at[d], to_z(zz), "pz", z, z_recv.at[z])
+        else:
+            total += keep[d] + x_recv[d].astype(f32)
+    for zz in arrivals:
+        arrived(z_recv.at[zz], "pz", zz)
+        total += z_recv[zz].astype(f32)
+    out_ref[...] = total.astype(bf16)
     for copy in started:
         copy.wait_send()
+
+    @pl.when(inner == 1)
+    def _():
+        for on in passed:
+            on.wait_send()
 
 
 def kernel_body(zn, *args):
@@ -517,35 +593,34 @@
      gate_weight, value_weight, conv_weight, down_weight) = args
     rows, width = residual.shape
     sub = down_weight.shape[0] // zn
-    share, half = rows // 4, rows // 2
+    share = rows // 4
     d_own = gate_weight.shape[0]
-    positions = lax.axis_index("sp") * rows + jnp.arange(rows, dtype=jnp.int32)
-    cos_table, sine_table = tables(positions, ROPE)
-    gain = norm_gain.reshape(width // rows, rows).astype(jnp.float32)
-    table = jnp.concatenate([cos_table.T, sine_table.T, gain], axis=0)
     bf16, f32 = jnp.bfloat16, jnp.float32
     vals = VAL_A + VAL_B
     lanes = -(-vals // 128) * 128
     halo_lanes = -(-sub // 128) * 128
     V, DMA = pltpu.VMEM, pltpu.SemaphoreType.DMA
-    sems = [DMA((6,))]
-    for count in (zn, zn, 2 * zn, zn, zn, zn, zn, 3, zn, zn, 2 * zn, 1, zn, zn, zn):
-        sems += [DMA((count,)), DMA((count,))]
     return pl.pallas_call(
         functools.partial(layer_kernel, zn),
         out_shape=jax.ShapeDtypeStruct((share, width), bf16),
-        in_specs=[pl.BlockSpec(memory_space=V)] * 5 + [pl.BlockSpec(memory_space=pl.ANY)] * 6,
+        in_specs=[pl.BlockSpec(memory_space=pl.ANY)] * 11,
         out_specs=pl.BlockSpec(memory_space=V),
         scratch_shapes=[
+            V((queries.shape[1], rows), bf16),
+            V(latents.shape, bf16),
+            V((ROPE, rows), bf16),
+            V(conv_weight.shape, bf16),
+            V((1, width), bf16),
             V(expand_weight.shape, bf16),
-            V((share, width), bf16),
+            V((2, share, width), bf16),
             V(out_weight.shape, bf16),
             V(gate_weight.shape, bf16),
             V(value_weight.shape, bf16),
             V(down_weight.shape, bf16),
-            V((2 * zn, 2, half, latents.shape[1] + 2 * ROPE), bf16),
-            V((4, share, lanes), bf16),
-            V((4, share, lanes), bf16),
+            V((2 * zn, 4, share // 2, 2 * latents.shape[1] + 2 * ROPE), bf16),
+            V((2, 2, share, lanes), bf16),
+            V((4, 2, share, lanes), bf16),
+            V((2, share, width), bf16),
             V((zn, 4, share, width), bf16),
             V((zn, d_own, 2 * sub), bf16),
             V((2 * zn, d_own, 2 * sub), bf16),
@@ -562,10 +637,13 @@
             V((zn, share, width), bf16),
             V((zn, share, width), bf16),
             V((zn, share, width), bf16),
-        ] + sems,
+            DMA((12,)),
+            DMA((SENDS,)),
+            DMA((len(KINDS) * zn,)),
+        ],
         compiler_params=pltpu.CompilerParams(collective_id=0, has_side_effects=True),
-    )(table, queries.T, latents, shared_key.T, conv_weight, expand_weight, residual, out_weight,
-      gate_weight, value_weight, down_weight)
+    )(queries.T, latents, shared_key.T, conv_weight, norm_gain.reshape(1, width), expand_weight, residual,
+      out_weight, gate_weight, value_weight, down_weight)
 
 
 def pick(*args):
@@ -573,7 +651,7 @@
     hidden = args[10].shape[0]
     sub = hidden // zn
     fits = (
-        lax.axis_size("sp") % 2 == 0
+        lax.axis_size("sp") == 8
         and lax.axis_size("tp") == 4
         and hidden % zn == 0
         and sub % 64 == 0

time: 91.4 us -> 83.5 us (0.914)
  Pallas kernels: 88.2 us -> 80.3 us
  other arithmetic: 1.47 us -> 0 us
  local copies, waits for them, and re-layouts: 1.57 us -> 2.86 us
    pallas_call x1, Pallas kernels: 88.2 us -> 80.3 us  [kernel_body(): pl.pallas_call(functools.partial(layer_kernel, zn), out_shape=jax.ShapeDt...]
    reshape x0 -> x1, local copies, waits for them, and re-layouts: none -> 1.29 us  [kernel_body(): norm_gain.reshape(1, width)]
where the time goes in v1:
time: 83.5 us; the launch traced here: 83.2 us
  Pallas kernels  80.3 us (96%)
  local copies, waits for them, and re-layouts  2.86 us (3%)
    pallas_call x1, Pallas kernels, kernel_body(): pl.pallas_call(functools.partial(layer_kernel, zn), out_shape=jax.ShapeDt...  80.3 us

profile of v1, /device:TPU:0, one launch (start us, length us, event | category | flops | bytes accessed | tf_op | source)
XLA Modules:
  0.0 83.2 jit_solution(985784885431285275)
XLA Ops:
  0.0 1.3 %reshape.3.gain_hbm = bf16[1,2048]{1,0:T(2,128)(2,1)} reshape(bf16[2048]{0:T(1024)(128)(2,1)} %param.17) | data formatting | bytes 8192 | tf_op jit(solution)/shard_map/reshape | solution.py:645
  1.3 80.3 %shard_map.109 = bf16[32,2048]{1,0:T(8,128)(2,1)} custom-call(bf16[320,128]{1,0:T(8,128)(2,1)} %bitcast.2, bf16[128,512]{1,0:T(8,128)(2,1)} %lat_hbm.1, bf16[64,128]{1,0:T(8,128)(2,1)} %bitcast.3, bf16[3,768]{1,0:T(4,128)(2,1)} %conv_hbm.1, bf16[1,2048]{1,0:T(2,128)(2,1)} %reshape.3.gain_hbm, bf16[512,384]{1,0:T(8,128)(2,1)} %expand_hbm.1, ...), custom_call_target="tpu_custom_call" | custom-call | tf_op jit(solution)/shard_map/pallas_call | solution.py:603
  81.6 1.6 %copy.13 = bf16[32,2048]{1,0:T(8,128)(2,1)} copy(bf16[32,2048]{1,0:T(8,128)(2,1)} %shard_map.109) | data formatting | bytes 262144

commit v2 on v1

--- a/solution.py
+++ b/solution.py
@@ -195,9 +195,10 @@
 MESH = pl.DeviceIdType.MESH
 KINDS = (
     "lz", "ly", "lx", "lxy", "lcz", "lcx", "lcy", "lcxy",
-    "wz", "wy", "dz", "dy", "nz", "nx", "ncz", "ncx", "at", "pc", "px", "pz", "h",
+    "wz", "", "wy", "", "dz", "dy", "nz", "", "nx", "", "ncz", "", "ncx", "",
+    "at", "pc", "h", "px", "", "", "", "pz", "", "", "",
 )
-SENDS = 96
+SENDS = 144
 
 
 def layer_kernel(
@@ -245,6 +246,7 @@
     x_recv,
     z_send,
     z_recv,
+    result,
     in_s,
     send_s,
     recv_s,
@@ -261,6 +263,7 @@
     rank = lat_ref.shape[1]
     sub = down_ref.shape[0] // zn
     sp = 2 * zn
+    deep = gate_ref.shape[0] // 2
 
     inner = ((z + 1) // 2) % 2
     near = z + 1 - 2 * (z % 2)
@@ -293,6 +296,21 @@
         copy = copy_to(ref, ref if dst is None else dst, dev, kind, i, new_slot())
         copy.start()
         started.append(copy)
+
+    def send_in(*turns):
+        slot = new_slot()
+
+        def start(which, ref, dev, kind, i, dst=None, wait=None):
+            @pl.when(turns[which])
+            def _():
+                if wait is not None:
+                    arrived(ref, wait, i)
+                copy_to(ref, ref if dst is None else dst, dev, kind, i, slot).start()
+
+            if which == 0:
+                started.append(copy_to(ref, ref if dst is None else dst, dev, kind, i, slot))
+
+        return start
 
     def arrived(dst, kind, i):
         with jax.named_scope("wait_" + kind):
@@ -348,8 +366,9 @@
     loads[2].wait()
     loads[3].wait()
     for k in range(zn):
-        stage[k, :, :sub] = gate_ref[:, k * sub : (k + 1) * sub]
-        stage[k, :, sub:] = value_ref[:, k * sub : (k + 1) * sub]
+        for i in range(2):
+            stage[k, i, :, :sub] = gate_ref[i * deep : (i + 1) * deep, k * sub : (k + 1) * sub]
+            stage[k, i, :, sub:] = value_ref[i * deep : (i + 1) * deep, k * sub : (k + 1) * sub]
     with jax.named_scope("barrier"):
         pl.semaphore_wait(barrier, len(partners))
 
@@ -360,8 +379,9 @@
         send(lat(z, y, t), to_z(zz), "lz", z)
     send(lat(z, y, t), y_dev, "ly", z)
     send(lat(z, y, xt), y_dev, "lxy", z)
-    for zz in (far, mid, near):
-        send(stage.at[zz], to_z(zz), "wz", z, w_full.at[s])
+    send(stage.at[near], to_z(near), "wz", 2 * z, w_full.at[s])
+    for zz, i in ((mid, 0), (mid, 1), (far, 0), (far, 1)):
+        send(stage.at[zz, i], to_z(zz), "wz", 2 * z + i, w_full.at[s, i])
     w_full[s] = stage[z]
 
     for zz in arrivals:
@@ -369,7 +389,6 @@
         send(lat(zz, y, t), y_dev, "ly", zz)
         send(lat(zz, y, t), x_dev, "lx", zz)
         send(lat(zz, y, t), c_dev, "lcz", zz)
-    send(w_full.at[s], y_dev, "wy", z)
     arrived(lat(z, yo, t), "ly", z)
     send(lat(z, yo, t), c_dev, "lcy", z)
     arrived(lat(z, yo, xt), "lxy", z)
@@ -383,6 +402,7 @@
         if i == 2:
             send(lat(zz, y, xt), y_dev, "lxy", zz)
         send(lat(zz, y, xt), c_dev, "lcx", zz)
+    send(w_full.at[s], y_dev, "wy", 2 * z)
 
     loads[4].wait()
     rot = NOPE_A + NOPE_B
@@ -446,13 +466,22 @@
     send(att_send.at[co], c_dev, "at", t, att_recv.at[t])
     att_recv[t] = att_send[c]
 
-    def forward_weights(zz):
-        arrived(w_full.at[2 * zz + y], "wz", zz)
-        send(w_full.at[2 * zz + y], y_dev, "wy", zz)
-
+    arrived(w_full.at[2 * near + y], "wz", 2 * near)
+    send(w_full.at[2 * near + y], y_dev, "wy", 2 * near)
+    first_on = inner * c == 1
+    weights_in = [
+        (k, i, send_in(first_on, (1 - inner * c) * (1 - i + i * inner) == 1, i * (1 - inner) == 1))
+        for k in (mid, far) for i in range(2)
+    ]
+
+    def forward_weights(which):
+        for zz, i, pass_on in weights_in:
+            if which < 2 or i == 1:
+                pass_on(which, w_full.at[2 * zz + y, i], y_dev, "wy", 2 * zz + i, wait="wz")
+
+    forward_weights(0)
     for load in loads[7:]:
         load.wait()
-    forward_weights(arrivals[0])
     for o in (ct, xt, xct):
         arrived(att_recv.at[o], "at", o)
 
@@ -466,53 +495,72 @@
     stream = (res_ref[...].reshape(2 * share, res_ref.shape[2]).astype(f32) + projected).astype(bf16)
     stream_f = stream.astype(f32)
     scaled = stream_f * lax.rsqrt(jnp.mean(stream_f * stream_f, axis=1, keepdims=True) + 1e-06)
-    normed = (scaled * gain_ref[...].astype(f32)).astype(bf16)
+    normed = (scaled * gain_ref[...].astype(f32).reshape(1, scaled.shape[1])).astype(bf16)
+    piece_rows = share // 2
     for i in range(2):
-        nrm[z, 2 * i + c] = normed[i * share : (i + 1) * share]
+        for j in range(2):
+            first = i * share + j * piece_rows
+            nrm[z, 2 * i + c, j] = normed[first : first + piece_rows]
         own_stream[i] = stream[i * share : (i + 1) * share]
 
-    own = nrm.at[z, t]
-    send(own, to_z(mid), "nz", z)
-    send(own, to_z(near), "nz", z)
-    send(own, c_dev, "ncz", z)
-    send(nrm.at[z, xt], c_dev, "ncx", z)
-
-    def send_down(zz):
-        piece = down_ref.at[pl.ds(pl.multiple_of(zz * sub, sub), sub), :]
-        send(piece, to_z(zz), "dz", z, dn_full.at[s])
-
-    send_down(far)
-    send_down(mid)
-    forward_weights(arrivals[1])
+    for j in range(2):
+        send(nrm.at[z, t, j], to_z(mid), "nz", 2 * z + j)
+        send(nrm.at[z, t, j], to_z(near), "nz", 2 * z + j)
+    send(nrm.at[z, t], c_dev, "ncz", 2 * z)
+    send(nrm.at[z, xt], c_dev, "ncx", 2 * z)
+    send(dn_full.at[s], y_dev, "dy", z)
+    forward_weights(1)
+
+    outer_turns = ((near, 0), (near, 1), (mid, 0), (far, 0), (mid, 1), (far, 1))
+    inner_turns = ((mid, 0), (far, 0), (mid, 1), (far, 1), (near, 0), (near, 1))
+    turns = [(a + inner * (b - a), i + inner * (j - i)) for (a, i), (b, j) in zip(outer_turns, inner_turns)]
+
+    def from_x(n):
+        zz, j = turns[n]
+        arrived(nrm.at[zz, xt, j], "nx", 2 * zz + j)
+        send(nrm.at[zz, xt, j], c_dev, "ncx", 2 * zz + j)
+
     passed = []
-    for i, zz in enumerate(arrivals):
-        blk = nrm.at[zz, t]
-        arrived(blk, "nz", zz)
-        if i < 2:
-            on = copy_to(blk, blk, to_z(near), "nz", zz, new_slot())
+    for n, (zz, j) in enumerate(turns):
+        blk = nrm.at[zz, t, j]
+        arrived(blk, "nz", 2 * zz + j)
+        if n < 4:
+            on = copy_to(blk, blk, to_z(near), "nz", 2 * zz + j, new_slot())
             passed.append(on)
 
             @pl.when(inner == 1)
             def _():
                 on.start()
 
-        send(blk, x_dev, "nx", zz)
-        send(blk, c_dev, "ncz", zz)
+        send(blk, x_dev, "nx", 2 * zz + j)
+        send(blk, c_dev, "ncz", 2 * zz + j)
+        if n == 1:
+            forward_weights(2)
+        if n > 1:
+            from_x(n - 2)
+    for zz in (near, mid, far):
+        piece = down_ref.at[pl.ds(pl.multiple_of(zz * sub, sub), sub), :]
+        send(piece, to_z(zz), "dz", z, dn_full.at[s])
+    from_x(len(turns) - 2)
+    from_x(len(turns) - 1)
+    for zz in (z, near):
+        arrived(w_full.at[2 * zz + yo], "wy", 2 * zz)
+    for zz, i, _ in weights_in:
+        arrived(w_full.at[2 * zz + yo, i], "wy", 2 * zz + i)
+    weights = w_full[...].reshape(sp * 2 * deep, 2 * sub)
+    def forward_down(zz):
+        arrived(dn_full.at[2 * zz + y], "dz", zz)
+        send(dn_full.at[2 * zz + y], y_dev, "dy", zz)
+
+    for i, zz in enumerate((z,) + arrivals):
         if i == 0:
-            forward_weights(arrivals[2])
-    send_down(near)
-    send(dn_full.at[s], y_dev, "dy", z)
-    for zz in (z,) + arrivals:
-        arrived(w_full.at[2 * zz + yo], "wy", zz)
-    weights = w_full[...].reshape(sp * w_full.shape[1], 2 * sub)
-    for i, zz in enumerate((z,) + arrivals):
-        if i > 0:
-            blk = nrm.at[zz, xt]
-            arrived(blk, "nx", zz)
-            send(blk, c_dev, "ncx", zz)
-        arrived(nrm.at[zz, ct], "ncz", zz)
-        arrived(nrm.at[zz, xct], "ncx", zz)
-        block = nrm[zz].reshape(rows, nrm.shape[3])
+            arrived(nrm.at[zz, ct], "ncz", 2 * zz)
+            arrived(nrm.at[zz, xct], "ncx", 2 * zz)
+        else:
+            for j in range(2):
+                arrived(nrm.at[zz, ct, j], "ncz", 2 * zz + j)
+                arrived(nrm.at[zz, xct, j], "ncx", 2 * zz + j)
+        block = nrm[zz].reshape(rows, nrm.shape[4])
         hbuf[zz] = jnp.dot(block, weights, preferred_element_type=f32).astype(bf16)
 
     wide_lanes = halo_send.shape[1]
@@ -522,12 +570,8 @@
         halo_send[zn + k : zn + k + 1, :] = g[0:1, :]
     send(halo_send, y_dev, "h", 0, halo_recv)
 
-    def forward_down(zz):
-        arrived(dn_full.at[2 * zz + y], "dz", zz)
-        send(dn_full.at[2 * zz + y], y_dev, "dy", zz)
-
-    for zz in arrivals:
-        forward_down(zz)
+    columns = (z, near, mid, far)
+    forward_down(near)
     conv_all = conv_ref[...].astype(f32)
     pieces = [conv_all[:, k * sub : (k + 1) * sub] for k in range(zn)]
     taps = pieces[0]
@@ -550,35 +594,63 @@
         v = hbuf[k].astype(f32)[:, sub:]
         abuf[k] = (mixed / (1.0 + jnp.exp(-mixed)) * v).astype(bf16)
 
-    for zz in (z,) + arrivals:
-        arrived(dn_full.at[2 * zz + yo], "dy", zz)
     order = (far, mid, near, z)
     depth = dn_full.shape[2]
-    for d, zz in enumerate(order):
-        a = abuf[zz]
-        for k in range(sp):
-            p = jnp.dot(a, dn_full[k], preferred_element_type=f32)
-            part[d, :, :, k * depth : (k + 1) * depth] = p.reshape(4, share, depth)
-        for i in range(2):
-            c_send[d, i] = part[d, 2 * i + co].astype(bf16)
-        send(c_send.at[d], c_dev, "pc", d, c_recv.at[d])
-    for d, zz in enumerate(order):
-        arrived(c_recv.at[d], "pc", d)
-        x_send[d] = (part[d, xt] + c_recv[d, xo].astype(f32)).astype(bf16)
-        send(x_send.at[d], x_dev, "px", d, x_recv.at[d])
-        keep[d] = part[d, t] + c_recv[d, x].astype(f32)
-    total = own_stream[x].astype(f32)
-    for d, zz in enumerate(order):
-        arrived(x_recv.at[d], "px", d)
-        if d < zn - 1:
-            z_send[d] = (keep[d] + x_recv[d].astype(f32)).astype(bf16)
-            send(z_send.at[d], to_z(zz), "pz", z, z_recv.at[z])
-        else:
-            total += keep[d] + x_recv[d].astype(f32)
-    for zz in arrivals:
-        arrived(z_recv.at[zz], "pz", zz)
-        total += z_recv[zz].astype(f32)
-    out_ref[...] = total.astype(bf16)
+    two = 2 * depth
+
+    def multiply(g):
+        zz = columns[g]
+        arrived(dn_full.at[2 * zz + yo], "dy", zz)
+        down = jnp.concatenate([dn_full[2 * zz], dn_full[2 * zz + 1]], axis=1)
+        for d, to in enumerate(order):
+            p = jnp.dot(abuf[to], down, preferred_element_type=f32)
+            part[g, d] = p.reshape(4, share, two)
+            for i in range(2):
+                c_send[g, d, i] = part[g, d, 2 * i + co].astype(bf16)
+        send(c_send.at[g], c_dev, "pc", g, c_recv.at[g])
+
+    def over_x(g):
+        arrived(c_recv.at[g], "pc", g)
+        for d in range(zn):
+            x_send[g, d] = (part[g, d, xt] + c_recv[g, d, xo].astype(f32)).astype(bf16)
+            send(x_send.at[g, d], x_dev, "px", g * zn + d, x_recv.at[g, d])
+            keep[g, d] = part[g, d, t] + c_recv[g, d, x].astype(f32)
+
+    def over_z(g):
+        for d, to in enumerate(order):
+            arrived(x_recv.at[g, d], "px", g * zn + d)
+            both = keep[g, d] + x_recv[g, d].astype(f32)
+            if d < zn - 1:
+                z_send[g, d] = both.astype(bf16)
+                send(z_send.at[g, d], to_z(to), "pz", columns[g] * zn + z, z_recv.at[columns[g], z])
+            else:
+                keep[g, d] = both
+
+    multiply(0)
+    forward_down(mid)
+    over_x(0)
+    multiply(1)
+    over_x(1)
+    over_z(0)
+    forward_down(far)
+    multiply(2)
+    over_x(2)
+    over_z(1)
+    multiply(3)
+    over_x(3)
+    over_z(2)
+    over_z(3)
+    leaving = []
+    for g, zz in enumerate(columns):
+        total = keep[g, zn - 1]
+        for frm in arrivals:
+            arrived(z_recv.at[zz, frm], "pz", zz * zn + frm)
+            total += z_recv[zz, frm].astype(f32)
+        where = pl.ds(pl.multiple_of(zz * two, two), two)
+        result[:, where] = (own_stream[x, :, where].astype(f32) + total).astype(bf16)
+        leave = pltpu.make_async_copy(result.at[:, where], out_ref.at[:, where], in_s.at[len(pairs) + g])
+        leave.start()
+        leaving.append(leave)
     for copy in started:
         copy.wait_send()
 
@@ -586,6 +658,9 @@
     def _():
         for on in passed:
             on.wait_send()
+
+    for leave in leaving:
+        leave.wait()
 
 
 def kernel_body(zn, *args):
@@ -595,6 +670,7 @@
     sub = down_weight.shape[0] // zn
     share = rows // 4
     d_own = gate_weight.shape[0]
+    group = 2 * down_weight.shape[1]
     bf16, f32 = jnp.bfloat16, jnp.float32
     vals = VAL_A + VAL_B
     lanes = -(-vals // 128) * 128
@@ -604,13 +680,13 @@
         functools.partial(layer_kernel, zn),
         out_shape=jax.ShapeDtypeStruct((share, width), bf16),
         in_specs=[pl.BlockSpec(memory_space=pl.ANY)] * 11,
-        out_specs=pl.BlockSpec(memory_space=V),
+        out_specs=pl.BlockSpec(memory_space=pl.ANY),
         scratch_shapes=[
             V((queries.shape[1], rows), bf16),
             V(latents.shape, bf16),
             V((ROPE, rows), bf16),
             V(conv_weight.shape, bf16),
-            V((1, width), bf16),
+            V((width,), bf16),
             V(expand_weight.shape, bf16),
             V((2, share, width), bf16),
             V(out_weight.shape, bf16),
@@ -621,28 +697,29 @@
             V((2, 2, share, lanes), bf16),
             V((4, 2, share, lanes), bf16),
             V((2, share, width), bf16),
-            V((zn, 4, share, width), bf16),
-            V((zn, d_own, 2 * sub), bf16),
-            V((2 * zn, d_own, 2 * sub), bf16),
+            V((zn, 4, 2, share // 2, width), bf16),
+            V((zn, 2, d_own // 2, 2 * sub), bf16),
+            V((2 * zn, 2, d_own // 2, 2 * sub), bf16),
             V((2 * zn, sub, down_weight.shape[1]), bf16),
             V((zn, rows, 2 * sub), bf16),
             V((zn, rows, sub), bf16),
             V((2 * zn, halo_lanes), f32),
             V((2 * zn, halo_lanes), f32),
-            V((zn, 4, share, width), f32),
-            V((zn, 2, share, width), bf16),
-            V((zn, 2, share, width), bf16),
-            V((zn, share, width), f32),
-            V((zn, share, width), bf16),
-            V((zn, share, width), bf16),
-            V((zn, share, width), bf16),
-            V((zn, share, width), bf16),
-            DMA((12,)),
+            V((zn, zn, 4, share, group), f32),
+            V((zn, zn, 2, share, group), bf16),
+            V((zn, zn, 2, share, group), bf16),
+            V((zn, zn, share, group), f32),
+            V((zn, zn, share, group), bf16),
+            V((zn, zn, share, group), bf16),
+            V((zn, zn, share, group), bf16),
+            V((zn, zn, share, group), bf16),
+            V((share, width), bf16),
+            DMA((12 + zn,)),
             DMA((SENDS,)),
             DMA((len(KINDS) * zn,)),
         ],
         compiler_params=pltpu.CompilerParams(collective_id=0, has_side_effects=True),
-    )(queries.T, latents, shared_key.T, conv_weight, norm_gain.reshape(1, width), expand_weight, residual,
+    )(queries.T, latents, shared_key.T, conv_weight, norm_gain, expand_weight, residual,
       out_weight, gate_weight, value_weight, down_weight)
 
 

time: 83.5 us -> 70.9 us (0.85)
  Pallas kernels: 80.3 us -> 69.1 us
  local copies, waits for them, and re-layouts: 2.86 us -> 1.57 us
    pallas_call x1, Pallas kernels: 80.3 us -> 69.1 us  [kernel_body(): pl.pallas_call(functools.partial(layer_kernel, zn), out_shape=jax.ShapeDt...]
    reshape x1 -> x0, local copies, waits for them, and re-layouts: 1.29 us -> none  [kernel_body(): norm_gain.reshape(1, width)]
where the time goes in v2:
time: 70.9 us; the launch traced here: 70.6 us
  Pallas kernels  69.1 us (97%)
  local copies, waits for them, and re-layouts  1.57 us (2%)
    pallas_call x1, Pallas kernels, kernel_body(): pl.pallas_call(functools.partial(layer_kernel, zn), out_shape=jax.ShapeDt...  69.1 us
    unnamed x1, local copies, waits for them, and re-layouts  1.57 us

profile of v2, /device:TPU:0, one launch (start us, length us, event | category | flops | bytes accessed | tf_op | source)
XLA Modules:
  0.0 70.6 jit_solution(14854616326817824484)
XLA Ops:
  0.0 69.1 %shard_map.109 = bf16[32,2048]{1,0:T(8,128)(2,1)} custom-call(bf16[320,128]{1,0:T(8,128)(2,1)} %bitcast.2, bf16[128,512]{1,0:T(8,128)(2,1)} %lat_hbm.1, bf16[64,128]{1,0:T(8,128)(2,1)} %bitcast.3, bf16[3,768]{1,0:T(4,128)(2,1)} %conv_hbm.1, bf16[2048]{0:T(1024)(128)(2,1)} %gain_hbm.1, bf16[512,384]{1,0:T(8,128)(2,1)} %expand_hbm.1, ...), custom_call_target="tpu_custom_call" | custom-call | tf_op jit(solution)/shard_map/pallas_call | solution.py:679
  69.1 1.6 %copy.13 = bf16[32,2048]{1,0:T(8,128)(2,1)} copy(bf16[32,2048]{1,0:T(8,128)(2,1)} %shard_map.109) | data formatting | bytes 262144

commit v3 on v2

--- a/solution.py
+++ b/solution.py
@@ -193,12 +193,19 @@
 
 
 MESH = pl.DeviceIdType.MESH
-KINDS = (
-    "lz", "ly", "lx", "lxy", "lcz", "lcx", "lcy", "lcxy",
-    "wz", "", "wy", "", "dz", "dy", "nz", "", "nx", "", "ncz", "", "ncx", "",
-    "at", "pc", "h", "px", "", "", "", "pz", "", "", "",
-)
-SENDS = 144
+SINGLE = ("lc", "wy", "at", "h", "pz")
+PER_Z = ("lz", "ly", "lx", "lxy", "dz", "dy", "nc", "pc")
+PER_HALF = ("wz", "nz", "nx")
+GROUPS = ("lat", "weights", "down", "own", "relay", "normed", "at", "h", "pc", "px", "pz")
+
+
+def semaphore_places(zn):
+    places, count = {}, 0
+    for kinds, width in ((SINGLE, 1), (PER_Z, zn), (PER_HALF, 2 * zn), (("px",), zn * zn)):
+        for kind in kinds:
+            places[kind] = count
+            count += width
+    return places, count
 
 
 def layer_kernel(
@@ -279,42 +286,30 @@
     c_dev = {"sp": s, "tp": ct}
     xc_dev = {"sp": s, "tp": xct}
 
-    started = []
-    used = [0]
-
-    def copy_to(src, dst, dev, kind, i, slot):
+    places, _ = semaphore_places(zn)
+
+    def copy_to(src, dst, dev, kind, i, group):
         return pltpu.make_async_remote_copy(
-            src_ref=src, dst_ref=dst, send_sem=send_s.at[slot],
-            recv_sem=recv_s.at[KINDS.index(kind) * zn + i], device_id=dev, device_id_type=MESH,
+            src_ref=src, dst_ref=dst, send_sem=send_s.at[GROUPS.index(group)],
+            recv_sem=recv_s.at[places[kind] + i], device_id=dev, device_id_type=MESH,
         )
 
-    def new_slot():
-        used[0] += 1
-        return used[0] - 1
-
-    def send(ref, dev, kind, i, dst=None):
-        copy = copy_to(ref, ref if dst is None else dst, dev, kind, i, new_slot())
-        copy.start()
-        started.append(copy)
-
-    def send_in(*turns):
-        slot = new_slot()
-
-        def start(which, ref, dev, kind, i, dst=None, wait=None):
-            @pl.when(turns[which])
-            def _():
-                if wait is not None:
-                    arrived(ref, wait, i)
-                copy_to(ref, ref if dst is None else dst, dev, kind, i, slot).start()
-
-            if which == 0:
-                started.append(copy_to(ref, ref if dst is None else dst, dev, kind, i, slot))
-
-        return start
+    def send(ref, dev, kind, i, group, dst=None):
+        copy_to(ref, ref if dst is None else dst, dev, kind, i, group).start()
+
+    def send_if(condition, ref, dev, kind, i, group, dst=None, wait=None):
+        @pl.when(condition)
+        def _():
+            if wait is not None:
+                arrived(ref, wait, i)
+            send(ref, dev, kind, i, group, dst)
 
     def arrived(dst, kind, i):
         with jax.named_scope("wait_" + kind):
-            copy_to(dst, dst, c_dev, kind, i, 0).wait_recv()
+            copy_to(dst, dst, c_dev, kind, i, "lat").wait_recv()
+
+    def all_sent(ref, group):
+        copy_to(ref, ref, c_dev, "lz", 0, group).wait_send()
 
     barrier = pltpu.get_barrier_semaphore()
     partners = [to_z(near), to_z(mid), to_z(far), y_dev, x_dev, c_dev, xc_dev]
@@ -363,46 +358,46 @@
         lat_all[s, i, :, 2 * rank :] = jnp.concatenate(
             [key_turned[i * share : i * share + packed], key_turned[i * share + packed : (i + 1) * share]], axis=1
         )
+    with jax.named_scope("barrier"):
+        pl.semaphore_wait(barrier, len(partners))
+
+    def lat(zz, yy, q):
+        return lat_all.at[2 * zz + yy, q]
+
+    for zz in (far, mid, near):
+        send(lat(z, y, t), to_z(zz), "lz", z, "lat")
+    send(lat(z, y, t), y_dev, "ly", z, "lat")
+    send(lat(z, y, xt), y_dev, "lxy", z, "lat")
     loads[2].wait()
     loads[3].wait()
     for k in range(zn):
         for i in range(2):
             stage[k, i, :, :sub] = gate_ref[i * deep : (i + 1) * deep, k * sub : (k + 1) * sub]
             stage[k, i, :, sub:] = value_ref[i * deep : (i + 1) * deep, k * sub : (k + 1) * sub]
-    with jax.named_scope("barrier"):
-        pl.semaphore_wait(barrier, len(partners))
-
-    def lat(zz, yy, q):
-        return lat_all.at[2 * zz + yy, q]
-
-    for zz in (far, mid, near):
-        send(lat(z, y, t), to_z(zz), "lz", z)
-    send(lat(z, y, t), y_dev, "ly", z)
-    send(lat(z, y, xt), y_dev, "lxy", z)
-    send(stage.at[near], to_z(near), "wz", 2 * z, w_full.at[s])
+    send(stage.at[near], to_z(near), "wz", 2 * z, "weights", w_full.at[s])
     for zz, i in ((mid, 0), (mid, 1), (far, 0), (far, 1)):
-        send(stage.at[zz, i], to_z(zz), "wz", 2 * z + i, w_full.at[s, i])
+        send(stage.at[zz, i], to_z(zz), "wz", 2 * z + i, "weights", w_full.at[s, i])
     w_full[s] = stage[z]
 
     for zz in arrivals:
         arrived(lat(zz, y, t), "lz", zz)
-        send(lat(zz, y, t), y_dev, "ly", zz)
-        send(lat(zz, y, t), x_dev, "lx", zz)
-        send(lat(zz, y, t), c_dev, "lcz", zz)
+        send(lat(zz, y, t), y_dev, "ly", zz, "lat")
+        send(lat(zz, y, t), x_dev, "lx", zz, "lat")
+        send(lat(zz, y, t), c_dev, "lc", 0, "lat")
     arrived(lat(z, yo, t), "ly", z)
-    send(lat(z, yo, t), c_dev, "lcy", z)
+    send(lat(z, yo, t), c_dev, "lc", 0, "lat")
     arrived(lat(z, yo, xt), "lxy", z)
-    send(lat(z, yo, xt), c_dev, "lcxy", z)
+    send(lat(z, yo, xt), c_dev, "lc", 0, "lat")
     for i, zz in enumerate(arrivals):
         arrived(lat(zz, yo, t), "ly", zz)
         if i < 2:
-            send(lat(zz, yo, t), x_dev, "lxy", zz)
-        send(lat(zz, yo, t), c_dev, "lcy", zz)
+            send(lat(zz, yo, t), x_dev, "lxy", zz, "lat")
+        send(lat(zz, yo, t), c_dev, "lc", 0, "lat")
         arrived(lat(zz, y, xt), "lx", zz)
         if i == 2:
-            send(lat(zz, y, xt), y_dev, "lxy", zz)
-        send(lat(zz, y, xt), c_dev, "lcx", zz)
-    send(w_full.at[s], y_dev, "wy", 2 * z)
+            send(lat(zz, y, xt), y_dev, "lxy", zz, "lat")
+        send(lat(zz, y, xt), c_dev, "lc", 0, "lat")
+    send(w_full.at[s], y_dev, "wy", 0, "weights")
 
     loads[4].wait()
     rot = NOPE_A + NOPE_B
@@ -418,13 +413,8 @@
 
     for zz in arrivals:
         arrived(lat(zz, yo, xt), "lxy", zz)
-        send(lat(zz, yo, xt), c_dev, "lcxy", zz)
-    for zz in arrivals:
-        arrived(lat(zz, y, ct), "lcz", zz)
-        arrived(lat(zz, y, xct), "lcx", zz)
-    for zz in (z,) + arrivals:
-        arrived(lat(zz, yo, ct), "lcy", zz)
-        arrived(lat(zz, yo, xct), "lcxy", zz)
+        send(lat(zz, yo, xt), c_dev, "lc", 0, "lat")
+    arrived(lat_all.at[pl.ds(0, sp - 1), pl.ds(0, 2)], "lc", 0)
 
     whole = lat_all[...].reshape(sp * 4 * packed, lat_all.shape[3])
     expand_w = expand_ref[...]
@@ -461,29 +451,30 @@
     for i in range(4):
         att_send[i % 2, i // 2, :, :VAL_A] = wide[i * share : (i + 1) * share, :]
         att_send[i % 2, i // 2, :, VAL_A:vals] = narrow[i * share : (i + 1) * share, :]
-    send(att_send.at[c], x_dev, "at", t, att_recv.at[t])
-    send(att_send.at[co], xc_dev, "at", t, att_recv.at[t])
-    send(att_send.at[co], c_dev, "at", t, att_recv.at[t])
+    send(att_send.at[c], x_dev, "at", 0, "at", att_recv.at[t])
+    send(att_send.at[co], xc_dev, "at", 0, "at", att_recv.at[t])
+    send(att_send.at[co], c_dev, "at", 0, "at", att_recv.at[t])
     att_recv[t] = att_send[c]
 
     arrived(w_full.at[2 * near + y], "wz", 2 * near)
-    send(w_full.at[2 * near + y], y_dev, "wy", 2 * near)
-    first_on = inner * c == 1
-    weights_in = [
-        (k, i, send_in(first_on, (1 - inner * c) * (1 - i + i * inner) == 1, i * (1 - inner) == 1))
-        for k in (mid, far) for i in range(2)
-    ]
-
-    def forward_weights(which):
-        for zz, i, pass_on in weights_in:
-            if which < 2 or i == 1:
-                pass_on(which, w_full.at[2 * zz + y, i], y_dev, "wy", 2 * zz + i, wait="wz")
+    send(w_full.at[2 * near + y], y_dev, "wy", 0, "weights")
+
+    def forward_weights(turn):
+        for zz in (mid, far):
+            for i in range(2):
+                turns = (inner * c, (1 - inner * c) * (1 - i + i * inner), i * (1 - inner))
+                if turn == 2 and i == 0:
+                    continue
+
+                @pl.when(turns[turn] == 1)
+                def _():
+                    arrived(w_full.at[2 * zz + y, i], "wz", 2 * zz + i)
+                    send(w_full.at[2 * zz + y, i], y_dev, "wy", 0, "weights")
 
     forward_weights(0)
     for load in loads[7:]:
         load.wait()
-    for o in (ct, xt, xct):
-        arrived(att_recv.at[o], "at", o)
+    arrived(att_recv.at[pl.ds(0, 3)], "at", 0)
 
     projected = None
     for i in range(4):
@@ -504,11 +495,11 @@
         own_stream[i] = stream[i * share : (i + 1) * share]
 
     for j in range(2):
-        send(nrm.at[z, t, j], to_z(mid), "nz", 2 * z + j)
-        send(nrm.at[z, t, j], to_z(near), "nz", 2 * z + j)
-    send(nrm.at[z, t], c_dev, "ncz", 2 * z)
-    send(nrm.at[z, xt], c_dev, "ncx", 2 * z)
-    send(dn_full.at[s], y_dev, "dy", z)
+        send(nrm.at[z, t, j], to_z(mid), "nz", 2 * z + j, "own")
+        send(nrm.at[z, t, j], to_z(near), "nz", 2 * z + j, "own")
+    send(nrm.at[z, t], c_dev, "nc", z, "own")
+    send(nrm.at[z, xt], c_dev, "nc", z, "own")
+    send(dn_full.at[s], y_dev, "dy", z, "down")
     forward_weights(1)
 
     outer_turns = ((near, 0), (near, 1), (mid, 0), (far, 0), (mid, 1), (far, 1))
@@ -518,60 +509,57 @@
     def from_x(n):
         zz, j = turns[n]
         arrived(nrm.at[zz, xt, j], "nx", 2 * zz + j)
-        send(nrm.at[zz, xt, j], c_dev, "ncx", 2 * zz + j)
-
-    passed = []
+        send(nrm.at[zz, xt, j], c_dev, "nc", zz, "normed")
+
+    def send_down(zz):
+        piece = down_ref.at[pl.ds(pl.multiple_of(zz * sub, sub), sub), :]
+        send(piece, to_z(zz), "dz", z, "down", dn_full.at[s])
+
     for n, (zz, j) in enumerate(turns):
         blk = nrm.at[zz, t, j]
         arrived(blk, "nz", 2 * zz + j)
         if n < 4:
-            on = copy_to(blk, blk, to_z(near), "nz", 2 * zz + j, new_slot())
-            passed.append(on)
-
-            @pl.when(inner == 1)
-            def _():
-                on.start()
-
-        send(blk, x_dev, "nx", 2 * zz + j)
-        send(blk, c_dev, "ncz", 2 * zz + j)
+            send_if(inner == 1, blk, to_z(near), "nz", 2 * zz + j, "relay")
+        send(blk, x_dev, "nx", 2 * zz + j, "normed")
+        send(blk, c_dev, "nc", zz, "normed")
         if n == 1:
             forward_weights(2)
         if n > 1:
             from_x(n - 2)
-    for zz in (near, mid, far):
-        piece = down_ref.at[pl.ds(pl.multiple_of(zz * sub, sub), sub), :]
-        send(piece, to_z(zz), "dz", z, dn_full.at[s])
-    from_x(len(turns) - 2)
-    from_x(len(turns) - 1)
-    for zz in (z, near):
-        arrived(w_full.at[2 * zz + yo], "wy", 2 * zz)
-    for zz, i, _ in weights_in:
-        arrived(w_full.at[2 * zz + yo, i], "wy", 2 * zz + i)
+    for to in (near, mid, far):
+        send_down(to)
+    arrived(w_full.at[pl.ds(0, zn)], "wy", 0)
     weights = w_full[...].reshape(sp * 2 * deep, 2 * sub)
+
     def forward_down(zz):
         arrived(dn_full.at[2 * zz + y], "dz", zz)
-        send(dn_full.at[2 * zz + y], y_dev, "dy", zz)
-
-    for i, zz in enumerate((z,) + arrivals):
-        if i == 0:
-            arrived(nrm.at[zz, ct], "ncz", 2 * zz)
-            arrived(nrm.at[zz, xct], "ncx", 2 * zz)
-        else:
-            for j in range(2):
-                arrived(nrm.at[zz, ct, j], "ncz", 2 * zz + j)
-                arrived(nrm.at[zz, xct, j], "ncx", 2 * zz + j)
-        block = nrm[zz].reshape(rows, nrm.shape[4])
-        hbuf[zz] = jnp.dot(block, weights, preferred_element_type=f32).astype(bf16)
+        send(dn_full.at[2 * zz + y], y_dev, "dy", zz, "down")
+
+    def mix(zz):
+        hbuf[zz] = jnp.dot(
+            nrm[zz].reshape(rows, nrm.shape[4]), weights, preferred_element_type=f32
+        ).astype(bf16)
+
+    def block_here(zz):
+        arrived(nrm.at[zz, pl.ds(0, 2)], "nc", zz)
+
+    columns = (z, near + inner * (mid - near), mid + inner * (near - mid), far)
+    block_here(z)
+    mix(z)
+    for i, zz in enumerate(arrivals):
+        if i > 0:
+            from_x(len(turns) - 3 + i)
+        block_here(zz)
+        mix(zz)
 
     wide_lanes = halo_send.shape[1]
     for k in range(zn):
         g = hbuf[k, :, :wide_lanes].astype(f32)
         halo_send[k : k + 1, :] = g[rows - 1 : rows, :]
         halo_send[zn + k : zn + k + 1, :] = g[0:1, :]
-    send(halo_send, y_dev, "h", 0, halo_recv)
-
-    columns = (z, near, mid, far)
-    forward_down(near)
+    send(halo_send, y_dev, "h", 0, "h", halo_recv)
+
+    forward_down(columns[1])
     conv_all = conv_ref[...].astype(f32)
     pieces = [conv_all[:, k * sub : (k + 1) * sub] for k in range(zn)]
     taps = pieces[0]
@@ -580,6 +568,7 @@
     taps = jnp.concatenate([taps, jnp.zeros((taps.shape[0], wide_lanes - sub), f32)], axis=1)
     row_id = lax.broadcasted_iota(jnp.int32, (rows, wide_lanes), 0)
     arrived(halo_recv, "h", 0)
+    forward_down(columns[2])
     nothing = jnp.zeros((1, wide_lanes), f32)
     for k in range(zn):
         before_low = halo_recv[k - 1 : k, :] if k > 0 else nothing
@@ -607,60 +596,67 @@
             part[g, d] = p.reshape(4, share, two)
             for i in range(2):
                 c_send[g, d, i] = part[g, d, 2 * i + co].astype(bf16)
-        send(c_send.at[g], c_dev, "pc", g, c_recv.at[g])
-
-    def over_x(g):
-        arrived(c_recv.at[g], "pc", g)
-        for d in range(zn):
+        send(c_send.at[g], c_dev, "pc", g, "pc", c_recv.at[g])
+
+    def over_x(g, turns):
+        for d in turns:
             x_send[g, d] = (part[g, d, xt] + c_recv[g, d, xo].astype(f32)).astype(bf16)
-            send(x_send.at[g, d], x_dev, "px", g * zn + d, x_recv.at[g, d])
+            send(x_send.at[g, d], x_dev, "px", g * zn + d, "px", x_recv.at[g, d])
             keep[g, d] = part[g, d, t] + c_recv[g, d, x].astype(f32)
 
-    def over_z(g):
-        for d, to in enumerate(order):
+    def over_z(g, turns):
+        for d in turns:
             arrived(x_recv.at[g, d], "px", g * zn + d)
             both = keep[g, d] + x_recv[g, d].astype(f32)
             if d < zn - 1:
                 z_send[g, d] = both.astype(bf16)
-                send(z_send.at[g, d], to_z(to), "pz", columns[g] * zn + z, z_recv.at[columns[g], z])
+                send(z_send.at[g, d], to_z(order[d]), "pz", 0, "pz", z_recv.at[columns[g], z])
             else:
                 keep[g, d] = both
 
-    multiply(0)
-    forward_down(mid)
-    over_x(0)
-    multiply(1)
-    over_x(1)
-    over_z(0)
-    forward_down(far)
-    multiply(2)
-    over_x(2)
-    over_z(1)
-    multiply(3)
-    over_x(3)
-    over_z(2)
-    over_z(3)
+    away, stay = range(zn - 1), range(zn - 1, zn)
+    for g in range(zn):
+        multiply(g)
+        if g == 0:
+            forward_down(far)
+        arrived(c_recv.at[g], "pc", g)
+        over_x(g, away)
+        if g > 0:
+            over_z(g - 1, away)
+    for g in range(zn):
+        over_x(g, stay)
+    over_z(zn - 1, away)
+    for g in range(zn):
+        over_z(g, stay)
     leaving = []
+    arrived(z_recv.at[:, pl.ds(0, zn - 1)], "pz", 0)
     for g, zz in enumerate(columns):
         total = keep[g, zn - 1]
         for frm in arrivals:
-            arrived(z_recv.at[zz, frm], "pz", zz * zn + frm)
             total += z_recv[zz, frm].astype(f32)
         where = pl.ds(pl.multiple_of(zz * two, two), two)
         result[:, where] = (own_stream[x, :, where].astype(f32) + total).astype(bf16)
         leave = pltpu.make_async_copy(result.at[:, where], out_ref.at[:, where], in_s.at[len(pairs) + g])
         leave.start()
         leaving.append(leave)
-    for copy in started:
-        copy.wait_send()
+    all_sent(lat_all.at[pl.ds(0, sp - 1)], "lat")
+    all_sent(w_full.at[pl.ds(0, sp - 1)], "weights")
+    all_sent(dn_full.at[pl.ds(0, sp - 1)], "down")
+    all_sent(nrm.at[0], "own")
+    all_sent(nrm.at[pl.ds(0, zn - 1), pl.ds(0, 3)], "normed")
+    all_sent(att_recv.at[pl.ds(0, 3)], "at")
+    all_sent(halo_send, "h")
+    all_sent(c_send, "pc")
+    all_sent(x_send, "px")
+    all_sent(z_send.at[:, pl.ds(0, zn - 1)], "pz")
 
     @pl.when(inner == 1)
     def _():
-        for on in passed:
-            on.wait_send()
-
-    for leave in leaving:
-        leave.wait()
+        all_sent(nrm.at[0, pl.ds(0, 2)], "relay")
+
+    with jax.named_scope("leave"):
+        for leave in leaving:
+            leave.wait()
 
 
 def kernel_body(zn, *args):
@@ -715,8 +711,8 @@
             V((zn, zn, share, group), bf16),
             V((share, width), bf16),
             DMA((12 + zn,)),
-            DMA((SENDS,)),
-            DMA((len(KINDS) * zn,)),
+            DMA((len(GROUPS),)),
+            DMA((semaphore_places(zn)[1],)),
         ],
         compiler_params=pltpu.CompilerParams(collective_id=0, has_side_effects=True),
     )(queries.T, latents, shared_key.T, conv_weight, norm_gain, expand_weight, residual,

time: 70.9 us -> 67.9 us (0.958)
  Pallas kernels: 69.1 us -> 66.1 us
    pallas_call x1, Pallas kernels: 69.1 us -> 66.1 us  [kernel_body(): pl.pallas_call(functools.partial(layer_kernel, zn), out_shape=jax.ShapeDt...]
where the time goes in v3:
time: 67.9 us; the launch traced here: 67.6 us
  Pallas kernels  66.1 us (97%)
  local copies, waits for them, and re-layouts  1.57 us (2%)
    pallas_call x1, Pallas kernels, kernel_body(): pl.pallas_call(functools.partial(layer_kernel, zn), out_shape=jax.ShapeDt...  66.1 us
    unnamed x1, local copies, waits for them, and re-layouts  1.57 us

profile of v3, /device:TPU:0, one launch (start us, length us, event | category | flops | bytes accessed | tf_op | source)
XLA Modules:
  0.0 67.6 jit_solution(3523868115271870423)
XLA Ops:
  0.0 66.1 %shard_map.109 = bf16[32,2048]{1,0:T(8,128)(2,1)} custom-call(bf16[320,128]{1,0:T(8,128)(2,1)} %bitcast.2, bf16[128,512]{1,0:T(8,128)(2,1)} %lat_hbm.1, bf16[64,128]{1,0:T(8,128)(2,1)} %bitcast.3, bf16[3,768]{1,0:T(4,128)(2,1)} %conv_hbm.1, bf16[2048]{0:T(1024)(128)(2,1)} %gain_hbm.1, bf16[512,384]{1,0:T(8,128)(2,1)} %expand_hbm.1, ...), custom_call_target="tpu_custom_call" | custom-call | tf_op jit(solution)/shard_map/pallas_call | solution.py:675
  66.1 1.6 %copy.13 = bf16[32,2048]{1,0:T(8,128)(2,1)} copy(bf16[32,2048]{1,0:T(8,128)(2,1)} %shard_map.109) | data formatting | bytes 262144

commit v4 on v3

--- a/solution.py
+++ b/solution.py
@@ -194,8 +194,8 @@
 
 MESH = pl.DeviceIdType.MESH
 SINGLE = ("lc", "wy", "at", "h", "pz")
-PER_Z = ("lz", "ly", "lx", "lxy", "dz", "dy", "nc", "pc")
-PER_HALF = ("wz", "nz", "nx")
+PER_Z = ("lz", "ly", "lx", "lxy", "dz", "dy", "nc")
+PER_HALF = ("wz", "nz", "nx", "pc")
 GROUPS = ("lat", "weights", "down", "own", "relay", "normed", "at", "h", "pc", "px", "pz")
 
 
@@ -511,9 +511,12 @@
         arrived(nrm.at[zz, xt, j], "nx", 2 * zz + j)
         send(nrm.at[zz, xt, j], c_dev, "nc", zz, "normed")
 
-    def send_down(zz):
+    def send_down(zz, cond):
         piece = down_ref.at[pl.ds(pl.multiple_of(zz * sub, sub), sub), :]
-        send(piece, to_z(zz), "dz", z, "down", dn_full.at[s])
+        if cond is None:
+            send(piece, to_z(zz), "dz", z, "down", dn_full.at[s])
+        else:
+            send_if(cond, piece, to_z(zz), "dz", z, "down", dn_full.at[s])
 
     for n, (zz, j) in enumerate(turns):
         blk = nrm.at[zz, t, j]
@@ -524,10 +527,13 @@
         send(blk, c_dev, "nc", zz, "normed")
         if n == 1:
             forward_weights(2)
+        if n == 3:
+            send_down(mid, ((1 - inner) * c) == 1)
         if n > 1:
             from_x(n - 2)
-    for to in (near, mid, far):
-        send_down(to)
+    send_down(near, None)
+    send_down(mid, ((1 - inner) * c) == 0)
+    send_down(far, None)
     arrived(w_full.at[pl.ds(0, zn)], "wy", 0)
     weights = w_full[...].reshape(sp * 2 * deep, 2 * sub)
 
@@ -566,7 +572,23 @@
     for k in range(1, zn):
         taps = jnp.where(z == k, pieces[k], taps)
     taps = jnp.concatenate([taps, jnp.zeros((taps.shape[0], wide_lanes - sub), f32)], axis=1)
-    row_id = lax.broadcasted_iota(jnp.int32, (rows, wide_lanes), 0)
+
+    def activate(k, first, count, before=None, after=None):
+        g = hbuf[k, first : first + count, :wide_lanes].astype(f32)
+        row_id = lax.broadcasted_iota(jnp.int32, (count, wide_lanes), 0)
+        up, down = pltpu.roll(g, 1, 0), pltpu.roll(g, count - 1, 0)
+        if before is not None:
+            up = jnp.where(row_id == 0, before, up)
+        if after is not None:
+            down = jnp.where(row_id == count - 1, after, down)
+        mixed = up * taps[0:1] + g * taps[1:2] + down * taps[2:3]
+        mixed = mixed[:, :sub]
+        v = hbuf[k, first : first + count].astype(f32)[:, sub:]
+        return (mixed / (1.0 + jnp.exp(-mixed)) * v).astype(bf16)
+
+    edge = rows // 8
+    for k in range(zn):
+        abuf[k] = activate(k, 0, rows)
     arrived(halo_recv, "h", 0)
     forward_down(columns[2])
     nothing = jnp.zeros((1, wide_lanes), f32)
@@ -575,13 +597,8 @@
         before = jnp.where(y == 0, before_low, halo_recv[k : k + 1, :])
         after_high = halo_recv[zn + k + 1 : zn + k + 2, :] if k < zn - 1 else nothing
         after = jnp.where(y == 0, halo_recv[zn + k : zn + k + 1, :], after_high)
-        g = hbuf[k, :, :wide_lanes].astype(f32)
-        up = jnp.where(row_id == 0, before, pltpu.roll(g, 1, 0))
-        down = jnp.where(row_id == rows - 1, after, pltpu.roll(g, rows - 1, 0))
-        mixed = up * taps[0:1] + g * taps[1:2] + down * taps[2:3]
-        mixed = mixed[:, :sub]
-        v = hbuf[k].astype(f32)[:, sub:]
-        abuf[k] = (mixed / (1.0 + jnp.exp(-mixed)) * v).astype(bf16)
+        abuf[k, :edge] = activate(k, 0, 2 * edge, before=before)[:edge]
+        abuf[k, rows - edge :] = activate(k, rows - 2 * edge, 2 * edge, after=after)[edge:]
 
     order = (far, mid, near, z)
     depth = dn_full.shape[2]
@@ -596,10 +613,14 @@
             part[g, d] = p.reshape(4, share, two)
             for i in range(2):
                 c_send[g, d, i] = part[g, d, 2 * i + co].astype(bf16)
-        send(c_send.at[g], c_dev, "pc", g, "pc", c_recv.at[g])
+            if d % 2 == 1:
+                ready = pl.ds(d - 1, 2)
+                send(c_send.at[g, ready], c_dev, "pc", 2 * g + d // 2, "pc", c_recv.at[g, ready])
 
     def over_x(g, turns):
         for d in turns:
+            if d % 2 == 0:
+                arrived(c_recv.at[g, pl.ds(d, 2)], "pc", 2 * g + d // 2)
             x_send[g, d] = (part[g, d, xt] + c_recv[g, d, xo].astype(f32)).astype(bf16)
             send(x_send.at[g, d], x_dev, "px", g * zn + d, "px", x_recv.at[g, d])
             keep[g, d] = part[g, d, t] + c_recv[g, d, x].astype(f32)
@@ -619,7 +640,6 @@
         multiply(g)
         if g == 0:
             forward_down(far)
-        arrived(c_recv.at[g], "pc", g)
         over_x(g, away)
         if g > 0:
             over_z(g - 1, away)

time: 67.9 us -> 66.5 us (0.979)
  Pallas kernels: 66.1 us -> 64.7 us
    pallas_call x1, Pallas kernels: 66.1 us -> 64.7 us  [kernel_body(): pl.pallas_call(functools.partial(layer_kernel, zn), out_shape=jax.ShapeDt...]
where the time goes in v4:
time: 66.5 us; the launch traced here: 66.2 us
  Pallas kernels  64.7 us (97%)
  local copies, waits for them, and re-layouts  1.57 us (2%)
    pallas_call x1, Pallas kernels, kernel_body(): pl.pallas_call(functools.partial(layer_kernel, zn), out_shape=jax.ShapeDt...  64.7 us
    unnamed x1, local copies, waits for them, and re-layouts  1.57 us

profile of v4, /device:TPU:0, one launch (start us, length us, event | category | flops | bytes accessed | tf_op | source)
XLA Modules:
  0.0 66.2 jit_solution(11827292481335829436)
XLA Ops:
  0.0 64.7 %shard_map.109 = bf16[32,2048]{1,0:T(8,128)(2,1)} custom-call(bf16[320,128]{1,0:T(8,128)(2,1)} %bitcast.2, bf16[128,512]{1,0:T(8,128)(2,1)} %lat_hbm.1, bf16[64,128]{1,0:T(8,128)(2,1)} %bitcast.3, bf16[3,768]{1,0:T(4,128)(2,1)} %conv_hbm.1, bf16[2048]{0:T(1024)(128)(2,1)} %gain_hbm.1, bf16[512,384]{1,0:T(8,128)(2,1)} %expand_hbm.1, ...), custom_call_target="tpu_custom_call" | custom-call | tf_op jit(solution)/shard_map/pallas_call | solution.py:695
  64.7 1.6 %copy.13 = bf16[32,2048]{1,0:T(8,128)(2,1)} copy(bf16[32,2048]{1,0:T(8,128)(2,1)} %shard_map.109) | data formatting | bytes 262144

commit v5 on v4

--- a/solution.py
+++ b/solution.py
@@ -193,10 +193,10 @@
 
 
 MESH = pl.DeviceIdType.MESH
-SINGLE = ("lc", "wy", "at", "h", "pz")
+SINGLE = ("lc", "lco", "wy", "at", "an", "h", "pz")
 PER_Z = ("lz", "ly", "lx", "lxy", "dz", "dy", "nc")
 PER_HALF = ("wz", "nz", "nx", "pc")
-GROUPS = ("lat", "weights", "down", "own", "relay", "normed", "at", "h", "pc", "px", "pz")
+GROUPS = ("lat", "lat_o", "weights", "down", "own", "relay", "normed", "at", "an", "h", "pc", "px", "pz")
 
 
 def semaphore_places(zn):
@@ -236,6 +236,8 @@
     lat_all,
     att_send,
     att_recv,
+    nar_send,
+    nar_recv,
     own_stream,
     nrm,
     stage,
@@ -354,20 +356,20 @@
     for i in range(4):
         for j in range(2):
             first = i * share + j * packed
-            lat_all[s, i, :, j * rank : (j + 1) * rank] = lat_ref[first : first + packed, :]
-        lat_all[s, i, :, 2 * rank :] = jnp.concatenate(
+            lat_all[z, y, i, :, j * rank : (j + 1) * rank] = lat_ref[first : first + packed, :]
+        lat_all[z, y, i, :, 2 * rank :] = jnp.concatenate(
             [key_turned[i * share : i * share + packed], key_turned[i * share + packed : (i + 1) * share]], axis=1
         )
     with jax.named_scope("barrier"):
         pl.semaphore_wait(barrier, len(partners))
 
     def lat(zz, yy, q):
-        return lat_all.at[2 * zz + yy, q]
+        return lat_all.at[zz, yy, q]
 
     for zz in (far, mid, near):
         send(lat(z, y, t), to_z(zz), "lz", z, "lat")
-    send(lat(z, y, t), y_dev, "ly", z, "lat")
-    send(lat(z, y, xt), y_dev, "lxy", z, "lat")
+    send(lat(z, y, t), y_dev, "ly", z, "lat_o")
+    send(lat(z, y, xt), y_dev, "lxy", z, "lat_o")
     loads[2].wait()
     loads[3].wait()
     for k in range(zn):
@@ -381,21 +383,21 @@
 
     for zz in arrivals:
         arrived(lat(zz, y, t), "lz", zz)
-        send(lat(zz, y, t), y_dev, "ly", zz, "lat")
+        send(lat(zz, y, t), y_dev, "ly", zz, "lat_o")
         send(lat(zz, y, t), x_dev, "lx", zz, "lat")
         send(lat(zz, y, t), c_dev, "lc", 0, "lat")
     arrived(lat(z, yo, t), "ly", z)
-    send(lat(z, yo, t), c_dev, "lc", 0, "lat")
+    send(lat(z, yo, t), c_dev, "lco", 0, "lat_o")
     arrived(lat(z, yo, xt), "lxy", z)
-    send(lat(z, yo, xt), c_dev, "lc", 0, "lat")
+    send(lat(z, yo, xt), c_dev, "lco", 0, "lat_o")
     for i, zz in enumerate(arrivals):
         arrived(lat(zz, yo, t), "ly", zz)
         if i < 2:
-            send(lat(zz, yo, t), x_dev, "lxy", zz, "lat")
-        send(lat(zz, yo, t), c_dev, "lc", 0, "lat")
+            send(lat(zz, yo, t), x_dev, "lxy", zz, "lat_o")
+        send(lat(zz, yo, t), c_dev, "lco", 0, "lat_o")
         arrived(lat(zz, y, xt), "lx", zz)
         if i == 2:
-            send(lat(zz, y, xt), y_dev, "lxy", zz, "lat")
+            send(lat(zz, y, xt), y_dev, "lxy", zz, "lat_o")
         send(lat(zz, y, xt), c_dev, "lc", 0, "lat")
     send(w_full.at[s], y_dev, "wy", 0, "weights")
 
@@ -411,50 +413,82 @@
     dn_full[s] = down_ref[pl.ds(pl.multiple_of(z * sub, sub), sub), :]
     loads[6].wait()
 
-    for zz in arrivals:
+    def pass_far(zz):
         arrived(lat(zz, yo, xt), "lxy", zz)
-        send(lat(zz, yo, xt), c_dev, "lc", 0, "lat")
-    arrived(lat_all.at[pl.ds(0, sp - 1), pl.ds(0, 2)], "lc", 0)
-
-    whole = lat_all[...].reshape(sp * 4 * packed, lat_all.shape[3])
+        send(lat(zz, yo, xt), c_dev, "lco", 0, "lat_o")
+
     expand_w = expand_ref[...]
-    expanded = jnp.concatenate(
-        [
-            jnp.dot(whole[:, j * rank : (j + 1) * rank], expand_w, preferred_element_type=f32).astype(bf16)
-            for j in range(2)
-        ],
-        axis=0,
-    )
-    keys_t = whole[:, 2 * rank :]
     empty = jnp.zeros((rows, ROPE), bf16)
-
-    def attend(qc, qt, kc, v, scale):
-        dims = (((1,), (1,)), ((), ()))
+    nb = NOPE_A + VAL_A
+    dims = (((1,), (1,)), ((), ()))
+
+    def score(qc, qt, kc, keys_t, scale):
         turned_scores = [
             lax.dot_general(jnp.concatenate(two, axis=1), keys_t, dims, preferred_element_type=f32)
             for two in ([qt, empty], [empty, qt])
         ]
-        scores = (
+        return (
             lax.dot_general(qc, kc, dims, preferred_element_type=f32) + jnp.concatenate(turned_scores, axis=1)
         ) * scale
+
+    def scored(yy):
+        whole = lat_all[:, yy].reshape(zn * 4 * packed, lat_all.shape[4])
+        expanded = jnp.concatenate(
+            [
+                jnp.dot(whole[:, j * rank : (j + 1) * rank], expand_w, preferred_element_type=f32).astype(bf16)
+                for j in range(2)
+            ],
+            axis=0,
+        )
+        keys_t = whole[:, 2 * rank :]
+        return (
+            score(q_wide, q_wide_t, expanded[:, :NOPE_A], keys_t, (NOPE_A + ROPE) ** -0.5),
+            expanded[:, NOPE_A:nb],
+            score(q_narrow, q_narrow_t, expanded[:, nb : nb + NOPE_B], keys_t, (NOPE_B + ROPE) ** -0.5),
+            expanded[:, nb + NOPE_B : nb + NOPE_B + VAL_B],
+        )
+
+    pass_far(arrivals[0])
+
+    @pl.when(c == 1)
+    def _():
+        pass_far(arrivals[1])
+        pass_far(arrivals[2])
+
+    arrived(lat_all.at[pl.ds(0, zn - 1), 0, pl.ds(0, 2)], "lc", 0)
+    here = scored(y)
+
+    @pl.when(c == 0)
+    def _():
+        pass_far(arrivals[1])
+        pass_far(arrivals[2])
+
+    arrived(lat_all.at[:, 0, pl.ds(0, 2)], "lco", 0)
+    there = scored(yo)
+
+    def attend(head):
+        scores = jnp.concatenate([here[2 * head], there[2 * head]], axis=1)
+        v = jnp.concatenate([here[2 * head + 1], there[2 * head + 1]], axis=0)
         w = jnp.exp(scores - jnp.max(scores, axis=1, keepdims=True))
         total = jnp.sum(w, axis=1, keepdims=True)
         return (jnp.dot(w.astype(bf16), v, preferred_element_type=f32) / total).astype(bf16)
 
-    nb = NOPE_A + VAL_A
-    wide = attend(q_wide, q_wide_t, expanded[:, :NOPE_A], expanded[:, NOPE_A:nb], (NOPE_A + ROPE) ** -0.5)
-    narrow = attend(
-        q_narrow, q_narrow_t, expanded[:, nb : nb + NOPE_B],
-        expanded[:, nb + NOPE_B : nb + NOPE_B + VAL_B], (NOPE_B + ROPE) ** -0.5,
-    )
+    def to_heads(sent, received, kind):
+        send(sent.at[c], x_dev, kind, 0, kind, received.at[t])
+        send(sent.at[co], xc_dev, kind, 0, kind, received.at[t])
+        send(sent.at[co], c_dev, kind, 0, kind, received.at[t])
+        received[t] = sent[c]
+
     vals = VAL_A + VAL_B
+    wide = attend(0)
     for i in range(4):
-        att_send[i % 2, i // 2, :, :VAL_A] = wide[i * share : (i + 1) * share, :]
-        att_send[i % 2, i // 2, :, VAL_A:vals] = narrow[i * share : (i + 1) * share, :]
-    send(att_send.at[c], x_dev, "at", 0, "at", att_recv.at[t])
-    send(att_send.at[co], xc_dev, "at", 0, "at", att_recv.at[t])
-    send(att_send.at[co], c_dev, "at", 0, "at", att_recv.at[t])
-    att_recv[t] = att_send[c]
+        att_send[i % 2, i // 2] = wide[i * share : (i + 1) * share, :]
+    to_heads(att_send, att_recv, "at")
+    narrow = attend(1)
+    for i in range(4):
+        part_rows = narrow[i * share : (i + 1) * share, :]
+        nar_send[i % 2, i // 2] = jnp.concatenate([part_rows[:packed], part_rows[packed:]], axis=1)
+    to_heads(nar_send, nar_recv, "an")
 
     arrived(w_full.at[2 * near + y], "wz", 2 * near)
     send(w_full.at[2 * near + y], y_dev, "wy", 0, "weights")
@@ -475,11 +509,13 @@
     for load in loads[7:]:
         load.wait()
     arrived(att_recv.at[pl.ds(0, 3)], "at", 0)
+    arrived(nar_recv.at[pl.ds(0, 3)], "an", 0)
 
     projected = None
     for i in range(4):
+        narrow = [nar_recv[i, j, :, k * VAL_B : (k + 1) * VAL_B] for j in range(2) for k in range(2)]
         term = jnp.dot(
-            att_recv[i].reshape(2 * share, att_recv.shape[3])[:, :vals],
+            jnp.concatenate([att_recv[i].reshape(2 * share, VAL_A), jnp.concatenate(narrow, axis=0)], axis=1),
             out_w_ref[i * vals : (i + 1) * vals, :], preferred_element_type=f32,
         )
         projected = term if projected is None else projected + term
@@ -497,6 +533,7 @@
     for j in range(2):
         send(nrm.at[z, t, j], to_z(mid), "nz", 2 * z + j, "own")
         send(nrm.at[z, t, j], to_z(near), "nz", 2 * z + j, "own")
+    send_if(inner == 1, nrm.at[z, t, 0], to_z(far), "nz", 2 * z + 0, "relay")
     send(nrm.at[z, t], c_dev, "nc", z, "own")
     send(nrm.at[z, xt], c_dev, "nc", z, "own")
     send(dn_full.at[s], y_dev, "dy", z, "down")
@@ -521,13 +558,13 @@
     for n, (zz, j) in enumerate(turns):
         blk = nrm.at[zz, t, j]
         arrived(blk, "nz", 2 * zz + j)
-        if n < 4:
+        if 0 < n < 4:
             send_if(inner == 1, blk, to_z(near), "nz", 2 * zz + j, "relay")
         send(blk, x_dev, "nx", 2 * zz + j, "normed")
         send(blk, c_dev, "nc", zz, "normed")
         if n == 1:
             forward_weights(2)
-        if n == 3:
+        if n == 2:
             send_down(mid, ((1 - inner) * c) == 1)
         if n > 1:
             from_x(n - 2)
@@ -659,12 +696,14 @@
         leave = pltpu.make_async_copy(result.at[:, where], out_ref.at[:, where], in_s.at[len(pairs) + g])
         leave.start()
         leaving.append(leave)
-    all_sent(lat_all.at[pl.ds(0, sp - 1)], "lat")
+    all_sent(lat_all.at[pl.ds(0, zn - 1), 0], "lat")
+    all_sent(lat_all.at[:, 0], "lat_o")
     all_sent(w_full.at[pl.ds(0, sp - 1)], "weights")
     all_sent(dn_full.at[pl.ds(0, sp - 1)], "down")
     all_sent(nrm.at[0], "own")
     all_sent(nrm.at[pl.ds(0, zn - 1), pl.ds(0, 3)], "normed")
     all_sent(att_recv.at[pl.ds(0, 3)], "at")
+    all_sent(nar_recv.at[pl.ds(0, 3)], "an")
     all_sent(halo_send, "h")
     all_sent(c_send, "pc")
     all_sent(x_send, "px")
@@ -688,8 +727,6 @@
     d_own = gate_weight.shape[0]
     group = 2 * down_weight.shape[1]
     bf16, f32 = jnp.bfloat16, jnp.float32
-    vals = VAL_A + VAL_B
-    lanes = -(-vals // 128) * 128
     halo_lanes = -(-sub // 128) * 128
     V, DMA = pltpu.VMEM, pltpu.SemaphoreType.DMA
     return pl.pallas_call(
@@ -709,9 +746,11 @@
             V(gate_weight.shape, bf16),
             V(value_weight.shape, bf16),
             V(down_weight.shape, bf16),
-            V((2 * zn, 4, share // 2, 2 * latents.shape[1] + 2 * ROPE), bf16),
-            V((2, 2, share, lanes), bf16),
-            V((4, 2, share, lanes), bf16),
+            V((zn, 2, 4, share // 2, 2 * latents.shape[1] + 2 * ROPE), bf16),
+            V((2, 2, share, VAL_A), bf16),
+            V((4, 2, share, VAL_A), bf16),
+            V((2, 2, share // 2, 2 * VAL_B), bf16),
+            V((4, 2, share // 2, 2 * VAL_B), bf16),
             V((2, share, width), bf16),
             V((zn, 4, 2, share // 2, width), bf16),
             V((zn, 2, d_own // 2, 2 * sub), bf16),

time: 66.5 us -> 66.3 us (level)
  no operation moved by 1% of the time
where the time goes in v5:
time: 66.3 us; the launch traced here: 66 us
  Pallas kernels  64.5 us (97%)
  local copies, waits for them, and re-layouts  1.57 us (2%)
    pallas_call x1, Pallas kernels, kernel_body(): pl.pallas_call(functools.partial(layer_kernel, zn), out_shape=jax.ShapeDt...  64.5 us
    unnamed x1, local copies, waits for them, and re-layouts  1.57 us

profile of v5, /device:TPU:0, one launch (start us, length us, event | category | flops | bytes accessed | tf_op | source)
XLA Modules:
  0.0 66.0 jit_solution(1191554330145345102)
XLA Ops:
  0.0 64.5 %shard_map.109 = bf16[32,2048]{1,0:T(8,128)(2,1)} custom-call(bf16[320,128]{1,0:T(8,128)(2,1)} %bitcast.2, bf16[128,512]{1,0:T(8,128)(2,1)} %lat_hbm.1, bf16[64,128]{1,0:T(8,128)(2,1)} %bitcast.3, bf16[3,768]{1,0:T(4,128)(2,1)} %conv_hbm.1, bf16[2048]{0:T(1024)(128)(2,1)} %gain_hbm.1, bf16[512,384]{1,0:T(8,128)(2,1)} %expand_hbm.1, ...), custom_call_target="tpu_custom_call" | custom-call | tf_op jit(solution)/shard_map/pallas_call | solution.py:732
  64.5 1.6 %copy.13 = bf16[32,2048]{1,0:T(8,128)(2,1)} copy(bf16[32,2048]{1,0:T(8,128)(2,1)} %shard_map.109) | data formatting | bytes 262144

commit v6 on v5

--- a/solution.py
+++ b/solution.py
@@ -562,7 +562,7 @@
             send_if(inner == 1, blk, to_z(near), "nz", 2 * zz + j, "relay")
         send(blk, x_dev, "nx", 2 * zz + j, "normed")
         send(blk, c_dev, "nc", zz, "normed")
-        if n == 1:
+        if n == 0:
             forward_weights(2)
         if n == 2:
             send_down(mid, ((1 - inner) * c) == 1)
@@ -693,7 +693,7 @@
             total += z_recv[zz, frm].astype(f32)
         where = pl.ds(pl.multiple_of(zz * two, two), two)
         result[:, where] = (own_stream[x, :, where].astype(f32) + total).astype(bf16)
-        leave = pltpu.make_async_copy(result.at[:, where], out_ref.at[:, where], in_s.at[len(pairs) + g])
+        leave = pltpu.make_async_copy(result.at[:, where], out_ref.at[:, where], in_s.at[g])
         leave.start()
         leaving.append(leave)
     all_sent(lat_all.at[pl.ds(0, zn - 1), 0], "lat")
@@ -769,7 +769,7 @@
             V((zn, zn, share, group), bf16),
             V((zn, zn, share, group), bf16),
             V((share, width), bf16),
-            DMA((12 + zn,)),
+            DMA((12,)),
             DMA((len(GROUPS),)),
             DMA((semaphore_places(zn)[1],)),
         ],

time: 66.3 us -> 66.3 us (level)
  no operation moved by 1% of the time
where the time goes in v6:
time: 66.3 us; the launch traced here: 66 us
  Pallas kernels  64.4 us (97%)
  local copies, waits for them, and re-layouts  1.57 us (2%)
    pallas_call x1, Pallas kernels, kernel_body(): pl.pallas_call(functools.partial(layer_kernel, zn), out_shape=jax.ShapeDt...  64.4 us
    unnamed x1, local copies, waits for them, and re-layouts  1.57 us

profile of v6, /device:TPU:0, one launch (start us, length us, event | category | flops | bytes accessed | tf_op | source)
XLA Modules:
  0.0 66.0 jit_solution(3639815922991045257)
XLA Ops:
  0.0 64.4 %shard_map.109 = bf16[32,2048]{1,0:T(8,128)(2,1)} custom-call(bf16[320,128]{1,0:T(8,128)(2,1)} %bitcast.2, bf16[128,512]{1,0:T(8,128)(2,1)} %lat_hbm.1, bf16[64,128]{1,0:T(8,128)(2,1)} %bitcast.3, bf16[3,768]{1,0:T(4,128)(2,1)} %conv_hbm.1, bf16[2048]{0:T(1024)(128)(2,1)} %gain_hbm.1, bf16[512,384]{1,0:T(8,128)(2,1)} %expand_hbm.1, ...), custom_call_target="tpu_custom_call" | custom-call | tf_op jit(solution)/shard_map/pallas_call | solution.py:732
  64.4 1.6 %copy.13 = bf16[32,2048]{1,0:T(8,128)(2,1)} copy(bf16[32,2048]{1,0:T(8,128)(2,1)} %shard_map.109) | data formatting | bytes 262144
